TPU v7x, 512 devices: a whole 4x4x16 slice. The times are simulated.
512 devices in a mesh: sp: 32 (over z, core), tp: 16 (over y, x).
Axes of the slice: x: 4, y: 4, z: 16, core: 2. Of those that a mesh axis runs over, the one named last changes fastest.
Arguments:
- receptance: bfloat16 [8192, 4096], P('sp', 'tp'), may hold values from -6 to 6
- key_vectors: bfloat16 [8192, 4096], P('sp', 'tp'), may hold values from -13 to 13
- value_vectors: bfloat16 [8192, 4096], P('sp', 'tp'), may hold values from -6 to 6
- decay_logits: bfloat16 [8192, 4096], P('sp', 'tp'), may hold values from -20 to 2
- rate_logits: bfloat16 [8192, 4096], P('sp', 'tp'), may hold values from -8 to 4
- gate_logits: bfloat16 [8192, 4096], P('sp', 'tp'), may hold values from -6 to 6
- group_gain: float32 [4096], P('tp'), may hold values from 0.1 to 1.9
- residual: bfloat16 [8192, 4096], P('sp', 'tp'), may hold values from -24 to 24
- mixer_out: bfloat16 [4096, 4096], P(None, 'tp'), may hold values from -0.09375 to 0.09375
- norm_gain: float32 [4096], P('tp'), may hold values from 0.1 to 1.9
- expert_ids: int32 [8192, 2], P('sp'), may hold values from 0 to 31, as said below
- route_weight: float32 [8192, 2], P('sp'), may hold values from 0.25 to 1
- expert_gate: bfloat16 [32, 4096, 1024], P('sp', 'tp'), may hold values from -0.09375 to 0.09375
- expert_up: bfloat16 [32, 4096, 1024], P('sp', 'tp'), may hold values from -0.09375 to 0.09375
- expert_down: bfloat16 [32, 1024, 4096], P('sp', None, 'tp'), may hold values from -0.1875 to 0.1875
Outputs:
- updated: bfloat16 [8192, 4096], P('sp', 'tp')
Inputs may be any that keep to these rules, and one draw needn't show every extreme that they name: `expert_ids`: the experts of a row are different and lie in one group of 8 consecutive experts. In the rows of one index of sp (aligned blocks of 256 rows) no expert is named by more than 32 rows, and in every such block some expert is named by exactly 32 rows.
All inputs are finite; a program needn't handle non-finite values.
Results may differ from a plain program's by a relative error of at most 0.013.
Values may be sent and summed in bfloat16 or wider, within the bound.
A program may use at most 64 MiB of HBM per device.

v0:
```python
import jax
import jax.numpy as jnp
from jax import lax
from jax.sharding import Mesh
from jax.sharding import PartitionSpec as P

D = 4096
HEAD = 64
SPAN = 32
SP = ("sp_0", "sp_1")


EPS_GROUP = 0.00064
EPS_NORM = 1e-06
HIGHEST = lax.Precision.HIGHEST


def neutral_like(shard, identity):
    return jax.tree.map(
        lambda part, zero: jnp.zeros_like(part) + jnp.asarray(zero, part.dtype), shard, identity
    )


def carried_in(shard, axes, combine, identity):
    before = start = neutral_like(shard, identity)
    so_far = shard
    for axis in reversed(axes):
        size, mine = (lax.axis_size(axis), lax.axis_index(axis))
        pieces = jax.tree.map(
            lambda part, kind: lax.all_gather(part.astype(kind), axis),
            so_far,
            (jnp.bfloat16, jnp.bfloat16),
        )
        inside, so_far = (start, start)
        for k in range(size):
            passed = k < mine
            so_far = combine(
                so_far, jax.tree.map(lambda part, own: part[k].astype(own.dtype), pieces, shard)
            )
            inside = jax.tree.map(lambda new, old: jnp.where(passed, new, old), so_far, inside)
        before = combine(inside, before)
    return before


def from_everyone(shard, axis):
    size = lax.axis_size(axis)
    return lax.all_to_all(
        jnp.broadcast_to(shard[None], (size, *shard.shape)), axis, 0, 0, tiled=True
    )


def joined_along(pieces, dim):
    dims = list(pieces.shape[1:])
    dims[dim] *= pieces.shape[0]
    return jnp.moveaxis(pieces, 0, dim).reshape(dims)


def gather_directly(shard, axis, dim):
    pieces = from_everyone(shard, axis)
    return joined_along(pieces, dim)


def of_everyone(shard, axis):
    everything = from_everyone(shard, axis)
    return jnp.sum(everything, axis=0)


def split_up(shard, dim, size):
    before, after = (shard.shape[:dim], shard.shape[dim + 1 :])
    return jnp.moveaxis(shard.reshape(*before, size, -1, *after), dim, 0)


def sent_and_summed(shard, axis, dim):
    size = lax.axis_size(axis)
    pieces = lax.all_to_all(split_up(shard, dim, size), axis, 0, 0, tiled=True)
    return jnp.sum(pieces.astype(jnp.float32), axis=0)


def exact_einsum(pattern, first_op, second_op):
    return jnp.einsum(pattern, first_op, second_op, precision=HIGHEST)


def block_pieces(recept, keyvec, valvec, logdec, unit_key, correction):
    span_len = recept.shape[1]
    cum_in = jnp.cumsum(logdec, axis=1)
    cum_ex = cum_in - logdec
    cum_end = cum_in[:, span_len - 1 :]
    growth = jnp.exp(-cum_in)
    r_scaled = recept * jnp.exp(cum_in)
    u_scaled = unit_key * jnp.exp(cum_ex)
    k_scaled = keyvec * growth
    c_scaled = correction * growth
    row_pos = lax.broadcasted_iota(jnp.int32, (span_len, span_len), 0)
    col_pos = lax.broadcasted_iota(jnp.int32, (span_len, span_len), 1)
    strict = (col_pos < row_pos).astype(jnp.float32)
    causal = (col_pos <= row_pos).astype(jnp.float32)
    key_pull = exact_einsum("bthn,bshn->bhts", u_scaled, k_scaled) * strict
    corr_pull = exact_einsum("bthn,bshn->bhts", u_scaled, c_scaled) * strict
    key_read = exact_einsum("bthn,bshn->bhts", r_scaled, k_scaled) * causal
    corr_read = exact_einsum("bthn,bshn->bhts", r_scaled, c_scaled) * causal
    system = corr_pull + jnp.eye(span_len, dtype=jnp.float32)
    right_local = exact_einsum("bhts,bshn->bhtn", key_pull, valvec)
    right_start = jnp.swapaxes(u_scaled, 1, 2)
    solved = jax.scipy.linalg.solve_triangular(
        system, jnp.concatenate([right_local, right_start], axis=-1), lower=True, unit_diagonal=True
    )
    channels = valvec.shape[-1]
    pulled_local = solved[..., :channels]
    reach_rows = solved[..., channels:]
    read_local = exact_einsum("bhts,bshn->bthn", key_read, valvec) - exact_einsum(
        "bhts,bhsn->bthn", corr_read, pulled_local
    )
    start_rows = r_scaled - exact_einsum("bhts,bhsn->bthn", corr_read, reach_rows)
    tail_decay = jnp.exp(cum_end - cum_in)
    c_tail = correction * tail_decay
    k_tail = keyvec * tail_decay
    keep_end = jnp.exp(cum_end[:, 0])
    block_map = keep_end[..., :, None] * jnp.eye(channels, dtype=jnp.float32) - exact_einsum(
        "bhtj,bthl->bhjl", reach_rows, c_tail
    )
    block_add = exact_einsum("bthi,bthl->bhil", valvec, k_tail) - exact_einsum(
        "bhti,bthl->bhil", pulled_local, c_tail
    )
    return (read_local, start_rows, block_map, block_add)


def time_mix(
    receptance, key_vectors, value_vectors, decay_logits, rate_logits, gate_logits, group_gain
):
    tokens_here, channels = receptance.shape
    heads_here = channels // HEAD
    block_shape = (tokens_here // SPAN, SPAN, heads_here, HEAD)

    def arrange(array):
        return array.astype(jnp.float32).reshape(block_shape)

    recept = arrange(receptance)
    keyvec = arrange(key_vectors)
    valvec = arrange(value_vectors)
    logdec = -jnp.exp(-jax.nn.softplus(-arrange(decay_logits)) - 0.5)
    unit_key = keyvec / jnp.sqrt(1.0 + jnp.sum(keyvec * keyvec, axis=-1, keepdims=True))
    correction = unit_key * jax.nn.sigmoid(arrange(rate_logits))
    read_local, start_rows, block_map, block_add = block_pieces(
        recept, keyvec, valvec, logdec, unit_key, correction
    )
    eye_heads = jnp.broadcast_to(jnp.eye(HEAD, dtype=jnp.float32), (heads_here, HEAD, HEAD))
    zero_heads = jnp.zeros((heads_here, HEAD, HEAD), jnp.float32)

    def advance(carried, inputs):
        local_state, product = carried
        step_map, step_add = inputs
        new_state = exact_einsum("hij,hjl->hil", local_state, step_map) + step_add
        new_product = exact_einsum("hij,hjl->hil", product, step_map)
        return ((new_state, new_product), (local_state, product))

    (device_add, device_map), (starts, products) = lax.scan(
        advance, (zero_heads, eye_heads), (block_map, block_add)
    )

    def compose(earlier, following):
        return (
            exact_einsum("hij,hjl->hil", earlier[0], following[0]),
            exact_einsum("hij,hjl->hil", earlier[1], following[0]) + following[1],
        )

    prefix = carried_in((device_map, device_add), SP, compose, (eye_heads, zero_heads))
    incoming = prefix[1]
    from_local = exact_einsum("bthj,bhij->bthi", start_rows, starts)
    through = exact_einsum("bthl,bhjl->bthj", start_rows, products)
    state_read = read_local + from_local + exact_einsum("bthj,hij->bthi", through, incoming)
    centred = state_read - jnp.mean(state_read, axis=-1, keepdims=True)
    scaled = centred * lax.rsqrt(jnp.mean(centred * centred, axis=-1, keepdims=True) + EPS_GROUP)
    gated_out = (
        scaled.reshape(tokens_here, channels)
        * group_gain[None, :]
        * jax.nn.sigmoid(gate_logits.astype(jnp.float32))
    )
    return gated_out.astype(jnp.bfloat16)


def local(
    receptance,
    key_vectors,
    value_vectors,
    decay_logits,
    rate_logits,
    gate_logits,
    group_gain,
    residual,
    mixer_out,
    norm_gain,
    expert_ids,
    route_weight,
    expert_gate,
    expert_up,
    expert_down,
):
    mixed_rows = time_mix(
        receptance, key_vectors, value_vectors, decay_logits, rate_logits, gate_logits, group_gain
    )
    tokens_here, features = residual.shape
    projected = jnp.dot(
        gather_directly(mixed_rows, "tp", 1), mixer_out, preferred_element_type=jnp.float32
    )
    midway = (residual.astype(jnp.float32) + projected).astype(jnp.bfloat16)
    midway_f = midway.astype(jnp.float32)
    squares = of_everyone(jnp.sum(midway_f * midway_f, axis=1), "tp")
    inv_rms = lax.rsqrt(squares / D + EPS_NORM)
    normed = (midway_f * norm_gain[None, :] * inv_rms[:, None]).astype(jnp.bfloat16)
    routes = expert_ids.shape[1]
    experts_all = lax.axis_size(SP) * expert_gate.shape[0]
    capacity = 2 * tokens_here * routes // experts_all
    flat_ids = expert_ids.reshape(-1)
    onehot = (flat_ids[:, None] == jnp.arange(experts_all, dtype=jnp.int32)[None, :]).astype(
        jnp.int32
    )
    earlier_count = jnp.sum((jnp.cumsum(onehot, axis=0) - onehot) * onehot, axis=1)
    slot_of = flat_ids * capacity + earlier_count
    owner_token = jnp.arange(tokens_here * routes, dtype=jnp.int32) // routes
    slot_table = (
        jnp.full((experts_all * capacity,), tokens_here, jnp.int32).at[slot_of].set(owner_token)
    )
    padded = jnp.concatenate([normed, jnp.zeros((1, features), jnp.bfloat16)], axis=0)
    outgoing = padded[slot_table].reshape(experts_all, capacity, features)
    arrived = lax.all_to_all(outgoing, SP, split_axis=0, concat_axis=0, tiled=True)
    arrived_rows = arrived.reshape(-1, features)
    paired = jnp.concatenate([expert_gate[0], expert_up[0]], axis=1)
    gate_up = sent_and_summed(
        jnp.dot(arrived_rows, paired, preferred_element_type=jnp.float32).astype(jnp.bfloat16),
        "tp",
        0,
    )
    half_width = paired.shape[1] // 2
    hidden = (jax.nn.silu(gate_up[:, :half_width]) * gate_up[:, half_width:]).astype(jnp.bfloat16)
    expert_res = jnp.dot(
        gather_directly(hidden, "tp", 0), expert_down[0], preferred_element_type=jnp.float32
    )
    returned = lax.all_to_all(
        expert_res.astype(jnp.bfloat16).reshape(-1, capacity, features),
        SP,
        split_axis=0,
        concat_axis=0,
        tiled=True,
    )
    picked = (
        returned.reshape(-1, features)[slot_of]
        .astype(jnp.float32)
        .reshape(tokens_here, routes, features)
    )
    routed_sum = jnp.sum(picked * route_weight[:, :, None], axis=1)
    return (midway_f + routed_sum).astype(jnp.bfloat16)


def solution(mesh):
    torus = Mesh(mesh.devices.reshape(16, 2, mesh.shape["tp"]), ("sp_0", "sp_1", "tp"))
    return jax.shard_map(
        local,
        mesh=torus,
        in_specs=(
            P(SP, "tp"),
            P(SP, "tp"),
            P(SP, "tp"),
            P(SP, "tp"),
            P(SP, "tp"),
            P(SP, "tp"),
            P("tp"),
            P(SP, "tp"),
            P(None, "tp"),
            P("tp"),
            P(SP, None),
            P(SP, None),
            P(SP, "tp", None),
            P(SP, "tp", None),
            P(SP, None, "tp"),
        ),
        out_specs=P(SP, "tp"),
        check_vma=False,
    )
```

profile of v0, /device:TPU:1, one launch (start us, length us, event | category | flops | bytes accessed | tf_op | source)
XLA Modules:
  0.0 452.3 jit_solution(2173442664199103637)
XLA Ops:
  12.5 2.0 reshape.226
  16.6 3.0 convolution_multiply_fusion.3
  26.6 80.2 %custom-call.4 = f32[8,4,1,32,32]{3,4,2,1,0:T(8,128)} custom-call(f32[8,4,1,32,32]{4,3,2,1,0:T(8,128)} %fusion.18), custom_call_target="InvertDiagBlocksLowerTriangular" | custom-call | tf_op jit(solution)/shard_map/jit(_solve_triangular)/vmap(vmap())/triangular_solve | solution.py:104
  112.8 2.8 convolution_subtract_fusion
  115.6 2.2 convolution_subtract_fusion.1
  117.8 24.8 %while.17 = (s32[]{:T(128)}, f32[4,64,64]{1,2,0:T(8,128)S(1)}, f32[4,64,64]{1,2,0:T(8,128)S(1)}, f32[8,4,64,64]{2,3,1,0:T(8,128)}, f32[8,4,64,64]{2,3,0,1:T(8,12...) while((s32[]{:T(128)}, f32[4,64,64]{1,2,0:T(8,128)S(1)}, ...), condition=%wide.region_3.4_spmd.clone, body=%wide.region_2.3_spmd.clone.sunk | while | flops 25214980 | bytes 1377915 | solution.py:156
  142.7 8.3 %all-gather.2 = bf16[8,64,64]{2,1,0:T(8,128)(2,1)S(1)} all-gather(bf16[4,64,64]{2,1,0:T(8,128)(2,1)S(1)} %copy.223), channel_id=4, replica_groups=mesh['sp_0'=16,'sp_1'=2,'tp'=16] {'sp_1'}, dimensions={0}, use_global_device_ids=true | all-gather | bytes 98304 | tf_op jit(solution)/shard_map/all_gather | solution.py:30
  151.2 1.9 all-gather
  153.9 29.5 %all-gather.1 = bf16[64,64,64]{2,1,0:T(8,128)(2,1)S(1)} all-gather(bf16[4,64,64]{2,1,0:T(8,128)(2,1)S(1)} %get-tuple-element.134), channel_id=3, replica_groups=mesh['sp_0'=16,'sp_1'=2,'tp'=16] {'sp_0'}, dimensions={0}, use_global_device_ids=true | all-gather | bytes 557056 | tf_op jit(solution)/shard_map/all_gather | solution.py:30
  183.4 26.2 %all-gather.3 = bf16[64,64,64]{2,1,0:T(8,128)(2,1)S(1)} all-gather(bf16[4,64,64]{2,1,0:T(8,128)(2,1)S(1)} %get-tuple-element.132), channel_id=5, replica_groups=mesh['sp_0'=16,'sp_1'=2,'tp'=16] {'sp_0'}, dimensions={0}, use_global_device_ids=true | all-gather | bytes 557056 | tf_op jit(solution)/shard_map/all_gather | solution.py:30
  219.7 7.0 %all-to-all-start = ((bf16[16,256,256]{1,2,0:T(8,128)(2,1)}), bf16[16,256,256]{1,2,0:T(8,128)(2,1)}, u32[]{:S(2)}, u32[]{:S(2)}) async-start(bf16[16,256,256]{1,2,0:T(8,128)(2,1)} %broadcast_in_dim.31), calls=%async_computation | async-start | bytes 4194304 | tf_op jit(solution)/shard_map/all_to_all | solution.py:47
  229.0 2.4 scatter_custom_fusion
  231.5 15.2 %all-to-all-done = bf16[16,256,256]{1,2,0:T(8,128)(2,1)} async-done(((bf16[16,256,256]{1,2,0:T(8,128)(2,1)}), bf16[16,256,256]{1,2,0:T(8,128)(2,1)}, u32[]{:S(2)}, u32[]{:S(2)}) %all-to-all-start) | async-done | bytes 2097184 | tf_op jit(solution)/shard_map/all_to_all | solution.py:47
  246.7 2.4 multiply_reduce_fusion.3
  249.8 3.5 all-to-all-start.1
  253.3 6.7 %all-to-all-done.1 = f32[16,1,256]{2,1,0:T(1,128)S(1)} async-done(((f32[16,1,256]{2,1,0:T(1,128)}), f32[16,1,256]{2,1,0:T(1,128)S(1)}, u32[]{:S(2)}, u32[]{:S(2)}) %all-to-all-start.1) | async-done | bytes 16416 | tf_op jit(solution)/shard_map/all_to_all | solution.py:47
  260.1 3.9 gather_fusion
  264.1 56.7 %all_to_all.31 = bf16[32,32,256]{2,1,0:T(8,128)(2,1)S(1)} all-to-all(bf16[32,32,256]{2,1,0:T(8,128)(2,1)S(1)} %bitcast.150), channel_id=1, replica_groups=mesh['sp_0'=16,'sp_1'=2,'tp'=16] {'sp_0','sp_1'}, dimensions={0} | all-to-all | bytes 1048576 | tf_op jit(solution)/shard_map/all_to_all | solution.py:225
  320.8 2.3 convolution_convert_fusion
  323.1 52.7 %all_to_all.32 = bf16[16,64,2048]{2,1,0:T(8,128)(2,1)S(1)} all-to-all(bf16[16,64,2048]{2,1,0:T(8,128)(2,1)S(1)} %bitcast.145), channel_id=1, replica_groups=mesh['sp_0'=16,'sp_1'=2,'tp'=16] {'tp'}, dimensions={0} | all-to-all | bytes 8388608 | tf_op jit(solution)/shard_map/all_to_all | solution.py:75
  376.9 30.5 %all_to_all.33 = bf16[16,64,1024]{2,1,0:T(8,128)(2,1)S(1)} all-to-all(bf16[16,64,1024]{2,1,0:T(8,128)(2,1)S(1)} %broadcast_in_dim.35), channel_id=1, replica_groups=mesh['sp_0'=16,'sp_1'=2,'tp'=16] {'tp'}, dimensions={0} | all-to-all | bytes 4194304 | tf_op jit(solution)/shard_map/all_to_all | solution.py:47
  409.0 6.2 %all-to-all-start.5 = ((bf16[32,32,256]{2,1,0:T(8,128)(2,1)}), bf16[32,32,256]{2,1,0:T(8,128)(2,1)S(1)}, u32[]{:S(2)}, u32[]{:S(2)}) async-start(bf16[32,32,256]{2,1,0:T(8,128)(2,1)} %bitcast.24), calls=%async_computation.5 | async-start | bytes 1048576 | tf_op jit(solution)/shard_map/all_to_all | solution.py:238
  415.3 33.4 %all-to-all-done.5 = bf16[32,32,256]{2,1,0:T(8,128)(2,1)S(1)} async-done(((bf16[32,32,256]{2,1,0:T(8,128)(2,1)}), bf16[32,32,256]{2,1,0:T(8,128)(2,1)S(1)}, u32[]{:S(2)}, u32[]{:S(2)}) %all-to-all-start.5) | async-done | bytes 524320 | tf_op jit(solution)/shard_map/all_to_all | solution.py:238
  448.7 1.9 gather_fusion.1
  (226 shorter events, 70.2 us)
Async XLA Ops:
  0.0 246.7 %copy-start = (bf16[4096,256]{1,0:T(8,128)(2,1)S(1)}, bf16[4096,256]{1,0:T(8,128)(2,1)}, u32[]{:S(2)}) copy-start(bf16[4096,256]{1,0:T(8,128)(2,1)} %param.25) | copy-start | bytes 6291460
  0.0 6.1 %copy-start.23 = (bf16[256,256]{1,0:T(8,128)(2,1)S(1)}, bf16[256,256]{1,0:T(8,128)(2,1)}, u32[]{:S(2)}) copy-start(bf16[256,256]{1,0:T(8,128)(2,1)} %param.19) | copy-start | bytes 393220
  0.0 6.2 %copy-start.24 = (bf16[256,256]{1,0:T(8,128)(2,1)S(1)}, bf16[256,256]{1,0:T(8,128)(2,1)}, u32[]{:S(2)}) copy-start(bf16[256,256]{1,0:T(8,128)(2,1)} %param.21) | copy-start | bytes 393220
  0.1 5.3 %copy-start.14 = (f32[64,64]{1,0:T(8,128)}, f32[64,64]{1,0:T(8,128)S(1)}, u32[]{:S(2)}) copy-start(f32[64,64]{1,0:T(8,128)S(1)} %fusion.99) | copy-start | bytes 49156
  14.5 5.1 %copy-start.6 = (f32[8,32,4,64]{3,2,1,0:T(4,128)S(1)}, f32[8,32,4,64]{3,2,1,0:T(4,128)}, u32[]{:S(2)}) copy-start(f32[8,32,4,64]{3,2,1,0:T(4,128)} %copy-done.5) | copy-start | bytes 786436
  14.5 5.1 %copy-start.11 = (f32[8,32,4,64]{3,2,1,0:T(4,128)S(1)}, f32[8,32,4,64]{3,2,1,0:T(4,128)}, u32[]{:S(2)}) copy-start(f32[8,32,4,64]{3,2,1,0:T(4,128)} %div.42) | copy-start | bytes 786436
  14.5 5.1 %copy-start.30 = (f32[8,32,4]{1,2,0:T(4,128)S(1)}, f32[8,32,4]{1,2,0:T(4,128)}, u32[]{:S(2)}) copy-start(f32[8,32,4]{1,2,0:T(4,128)} %copy.207) | copy-start | bytes 12292
  16.6 4.4 copy-start.21
  19.6 3.3 copy-start.20
  21.0 3.7 copy-start.3
  21.0 3.7 copy-start.27
  21.0 3.7 copy-start.28
  21.0 3.7 copy-start.31
  22.9 83.8 %copy-start.22 = (f32[8,4,64]{2,1,0:T(4,128)S(1)}, f32[8,4,64]{2,1,0:T(4,128)}, u32[]{:S(2)}) copy-start(f32[8,4,64]{2,1,0:T(4,128)} %copy-done.21) | copy-start | bytes 24580
  112.8 5.0 %copy-start.25 = (f32[64,64]{0,1:T(8,128)S(1)}, f32[64,64]{0,1:T(8,128)}, u32[]{:S(2)}) copy-start(f32[64,64]{0,1:T(8,128)} %copy.246) | copy-start | bytes 49156
  219.7 7.0 %copy-start.32 = (s32[256,2]{0,1:T(2,128)S(1)}, s32[256,2]{0,1:T(2,128)}, u32[]{:S(2)}) copy-start(s32[256,2]{0,1:T(2,128)} %param.27) | copy-start | bytes 6148
  219.7 27.0 %copy-start.37 = (bf16[256,256]{1,0:T(8,128)(2,1)S(1)}, bf16[256,256]{1,0:T(8,128)(2,1)}, u32[]{:S(2)}) copy-start(bf16[256,256]{1,0:T(8,128)(2,1)} %param.24) | copy-start | bytes 393220
  219.7 27.0 %all-to-all-start = ((bf16[16,256,256]{1,2,0:T(8,128)(2,1)}), bf16[16,256,256]{1,2,0:T(8,128)(2,1)}, u32[]{:S(2)}, u32[]{:S(2)}) async-start(bf16[16,256,256]{1,2,0:T(8,128)(2,1)} %broadcast_in_dim.31), calls=%async_computation | async-start | bytes 4194304 | tf_op jit(solution)/shard_map/all_to_all | solution.py:47
  246.7 13.3 %copy-start.35 = (f32[256]{0:T(256)S(1)}, f32[256]{0:T(256)}, u32[]{:S(2)}) copy-start(f32[256]{0:T(256)} %param.26) | copy-start | bytes 3076
  249.8 10.2 %all-to-all-start.1 = ((f32[16,1,256]{2,1,0:T(1,128)}), f32[16,1,256]{2,1,0:T(1,128)S(1)}, u32[]{:S(2)}, u32[]{:S(2)}) async-start(f32[16,1,256]{2,1,0:T(1,128)} %broadcast_in_dim.32), calls=%async_computation.1 | async-start | bytes 32768 | tf_op jit(solution)/shard_map/all_to_all | solution.py:47
  260.1 60.7 %copy-start.19 = (bf16[1,256,1024]{2,1,0:T(8,128)(2,1)S(1)}, bf16[1,256,1024]{2,1,0:T(8,128)(2,1)}, u32[]{:S(2)}) copy-start(bf16[1,256,1024]{2,1,0:T(8,128)(2,1)} %param.30) | copy-start | bytes 1572868
  376.9 30.5 %copy-start.36 = (bf16[1,1024,256]{2,1,0:T(8,128)(2,1)S(1)}, bf16[1,1024,256]{2,1,0:T(8,128)(2,1)}, u32[]{:S(2)}) copy-start(bf16[1,1024,256]{2,1,0:T(8,128)(2,1)} %param.31) | copy-start | bytes 1572868
  407.4 7.7 %copy-start.33 = (f32[256,2]{0,1:T(2,128)S(1)}, f32[256,2]{0,1:T(2,128)}, u32[]{:S(2)}) copy-start(f32[256,2]{0,1:T(2,128)} %param.28) | copy-start | bytes 6148
  409.0 39.7 %all-to-all-start.5 = ((bf16[32,32,256]{2,1,0:T(8,128)(2,1)}), bf16[32,32,256]{2,1,0:T(8,128)(2,1)S(1)}, u32[]{:S(2)}, u32[]{:S(2)}) async-start(bf16[32,32,256]{2,1,0:T(8,128)(2,1)} %bitcast.24), calls=%async_computation.5 | async-start | bytes 1048576 | tf_op jit(solution)/shard_map/all_to_all | solution.py:238
  (17 other events, 31.5 us)
where the time goes:
time: 453 us; the launch traced here: 452 us
  blocking collectives  206 us (45%)
  other arithmetic  96.4 us (21%)
  waiting for transfers between devices  55.2 us (12%)
  matrix products  46.5 us (10%)
  local copies, waits for them, and re-layouts  30.4 us (7%)
  starting transfers between devices  16.6 us (4%)
    another operation x3, other arithmetic, block_pieces(): jax.scipy.linalg.solve_triangular(system, jnp.concatenate([right_local, r...  80.9 us
    all_gather x4, blocking collectives, carried_in(): lax.all_gather(part.astype(kind), axis)  65.9 us
    all_to_all x1, blocking collectives, local(): lax.all_to_all(outgoing, SP, split_axis=0, concat_axis=0, tiled=True)  56.7 us
    all_to_all x1, blocking collectives, sent_and_summed(): pieces = lax.all_to_all(split_up(shard, dim, size), axis, 0, 0, tiled=True)  52.7 us
    dot_general x53, matrix products, exact_einsum(): return jnp.einsum(pattern, first_op, second_op, precision=HIGHEST)  39.1 us
    all_to_all x1, waiting for transfers between devices, local(): lax.all_to_all(expert_res.astype(jnp.bfloat16).reshape(-1, capacity, feat...  33.4 us
    all_to_all x1, blocking collectives, from_everyone(): lax.all_to_all(jnp.broadcast_to(shard[None], (size, *shard.shape)), axis,...  30.5 us
    all_to_all x2, waiting for transfers between devices, from_everyone(): lax.all_to_all(jnp.broadcast_to(shard[None], (size, *shard.shape)), axis,...  21.9 us
  transfers between devices with their start and end apart: 3, of which 3 were waited for; matrix products, arithmetic and copies ran while one was open for 1% of the time, Pallas kernels for 0%

commit v1 on v0

--- a/solution.py
+++ b/solution.py
@@ -1,12 +1,13 @@
 import jax
 import jax.numpy as jnp
 from jax import lax
+from jax.experimental import pallas as pl
+from jax.experimental.pallas import tpu as pltpu
 from jax.sharding import Mesh
 from jax.sharding import PartitionSpec as P
 
 D = 4096
 HEAD = 64
-SPAN = 32
 SP = ("sp_0", "sp_1")
 
 
@@ -80,48 +81,164 @@
     return jnp.einsum(pattern, first_op, second_op, precision=HIGHEST)
 
 
-def block_pieces(recept, keyvec, valvec, logdec, unit_key, correction):
-    span_len = recept.shape[1]
-    cum_in = jnp.cumsum(logdec, axis=1)
-    cum_ex = cum_in - logdec
-    cum_end = cum_in[:, span_len - 1 :]
-    growth = jnp.exp(-cum_in)
-    r_scaled = recept * jnp.exp(cum_in)
-    u_scaled = unit_key * jnp.exp(cum_ex)
-    k_scaled = keyvec * growth
-    c_scaled = correction * growth
-    row_pos = lax.broadcasted_iota(jnp.int32, (span_len, span_len), 0)
-    col_pos = lax.broadcasted_iota(jnp.int32, (span_len, span_len), 1)
-    strict = (col_pos < row_pos).astype(jnp.float32)
-    causal = (col_pos <= row_pos).astype(jnp.float32)
-    key_pull = exact_einsum("bthn,bshn->bhts", u_scaled, k_scaled) * strict
-    corr_pull = exact_einsum("bthn,bshn->bhts", u_scaled, c_scaled) * strict
-    key_read = exact_einsum("bthn,bshn->bhts", r_scaled, k_scaled) * causal
-    corr_read = exact_einsum("bthn,bshn->bhts", r_scaled, c_scaled) * causal
-    system = corr_pull + jnp.eye(span_len, dtype=jnp.float32)
-    right_local = exact_einsum("bhts,bshn->bhtn", key_pull, valvec)
-    right_start = jnp.swapaxes(u_scaled, 1, 2)
-    solved = jax.scipy.linalg.solve_triangular(
-        system, jnp.concatenate([right_local, right_start], axis=-1), lower=True, unit_diagonal=True
-    )
-    channels = valvec.shape[-1]
-    pulled_local = solved[..., :channels]
-    reach_rows = solved[..., channels:]
-    read_local = exact_einsum("bhts,bshn->bthn", key_read, valvec) - exact_einsum(
-        "bhts,bhsn->bthn", corr_read, pulled_local
-    )
-    start_rows = r_scaled - exact_einsum("bhts,bhsn->bthn", corr_read, reach_rows)
-    tail_decay = jnp.exp(cum_end - cum_in)
-    c_tail = correction * tail_decay
-    k_tail = keyvec * tail_decay
-    keep_end = jnp.exp(cum_end[:, 0])
-    block_map = keep_end[..., :, None] * jnp.eye(channels, dtype=jnp.float32) - exact_einsum(
-        "bhtj,bthl->bhjl", reach_rows, c_tail
-    )
-    block_add = exact_einsum("bthi,bthl->bhil", valvec, k_tail) - exact_einsum(
-        "bhti,bthl->bhil", pulled_local, c_tail
-    )
-    return (read_local, start_rows, block_map, block_add)
+F32 = jnp.float32
+BF16 = jnp.bfloat16
+CHUNK = 64
+
+
+def iota2(shape, dim):
+    return lax.broadcasted_iota(jnp.int32, shape, dim)
+
+
+def halves(x):
+    hi = x.astype(BF16)
+    return hi, (x - hi.astype(F32)).astype(BF16)
+
+
+def dot_dims(a, b, dims):
+    return lax.dot_general(a, b, (dims, ((), ())), preferred_element_type=F32)
+
+
+NN = ((1,), (0,))
+NT = ((1,), (1,))
+TN = ((0,), (0,))
+
+
+def both_rows(x):
+    hi, lo = halves(x)
+    return jnp.concatenate([hi, lo], axis=0)
+
+
+def left_split(a, b, dims=NN):
+    rows = a.shape[0]
+    full = dot_dims(both_rows(a), b, dims)
+    return full[:rows] + full[rows:]
+
+
+def two_split(a, b_hi, b_lo, dims=NN):
+    rows = a.shape[0]
+    hi, lo = halves(a)
+    full = dot_dims(jnp.concatenate([hi, lo], axis=0), b_hi, dims)
+    return full[:rows] + full[rows:] + dot_dims(hi, b_lo, dims)
+
+
+def block_diag(x, mask):
+    return jnp.concatenate([x] * (mask.shape[0] // x.shape[0]), axis=0) * mask
+
+
+def block_dot(a, b, mask, dims=NN):
+    b_hi, b_lo = halves(b)
+    return two_split(a, block_diag(b_hi, mask), block_diag(b_lo, mask), dims)
+
+
+def mix_body(r_ref, k_ref, v_ref, d_ref, b_ref, rd_ref, th_ref, ma_ref):
+    tokens, width = r_ref.shape
+    n = tokens // CHUNK
+    row = iota2((width, width), 0)
+    col = iota2((width, width), 1)
+    same = (row // CHUNK) == (col // CHUNK)
+    mask = same.astype(F32).astype(BF16)
+    diag = row == col
+    pos_t = iota2((CHUNK, width), 0)
+    pos_s = iota2((CHUNK, width), 1) % CHUNK
+    strict = pos_s < pos_t
+    causal = pos_s <= pos_t
+    eye_cat = (pos_s == pos_t).astype(F32)
+    tri = (iota2((CHUNK, CHUNK), 1) <= iota2((CHUNK, CHUNK), 0)).astype(F32).astype(BF16)
+    st = []
+    for c in range(n):
+        rows = pl.ds(c * CHUNK, CHUNK)
+        recept = r_ref[rows, :].astype(F32)
+        keyvec = k_ref[rows, :].astype(F32)
+        val = v_ref[rows, :]
+        logdec = (-0.6065306597126334) / (1.0 + jnp.exp(-d_ref[rows, :].astype(F32)))
+        rate = 1.0 / (1.0 + jnp.exp(-b_ref[rows, :].astype(F32)))
+        sums = left_split(keyvec * keyvec, mask)
+        unit = keyvec * lax.rsqrt(1.0 + sums)
+        corr = unit * rate
+        ld_hi, ld_lo = halves(logdec)
+        cum_in = dot_dims(tri, ld_hi, NN) + dot_dims(tri, ld_lo, NN)
+        cum_ex = cum_in - logdec
+        cum_end = cum_in[CHUNK - 1 : CHUNK, :]
+        growth = jnp.exp(-cum_in)
+        tail = jnp.exp(cum_end - cum_in)
+        r_s = recept * jnp.exp(cum_in)
+        u_s = unit * jnp.exp(cum_ex)
+        st.append(dict(val=val, r_s=r_s, u_s=u_s, k_s=keyvec * growth, c_s=corr * growth,
+                       c_tail=corr * tail, k_tail=keyvec * tail, keep=jnp.exp(cum_end)))
+    for q in st:
+        ur = jnp.concatenate([q["u_s"], q["r_s"]], axis=0)
+        g_k = block_dot(ur, q["k_s"], mask, NT)
+        g_c = block_dot(ur, q["c_s"], mask, NT)
+        q["key_pull"] = jnp.where(strict, g_k[:CHUNK], 0.0)
+        q["key_read"] = jnp.where(causal, g_k[CHUNK:], 0.0)
+        q["low"] = jnp.where(strict, g_c[:CHUNK], 0.0)
+        q["corr_read"] = jnp.where(causal, g_c[CHUNK:], 0.0)
+        first = ((pos_t // 2) == (pos_s // 2)) & (pos_s < pos_t)
+        q["x"] = eye_cat - jnp.where(first, q["low"], 0.0)
+    size = 2
+    while size < CHUNK:
+        level = ((pos_t // (2 * size)) == (pos_s // (2 * size))) & ((pos_t // size) > (pos_s // size))
+        for q in st:
+            q["t"] = block_dot(q["x"], jnp.where(level, q["low"], 0.0), mask)
+        for q in st:
+            q["x"] = q["x"] - block_dot(q["t"], q["x"], mask)
+        size *= 2
+    for q in st:
+        rl = left_split(jnp.concatenate([q["key_pull"], q["key_read"]], axis=0),
+                        block_diag(q["val"], mask))
+        q["right"], q["read"] = rl[:CHUNK], rl[CHUNK:]
+    for q in st:
+        q["pulled"] = block_dot(q["x"], q["right"], mask)
+        q["reach"] = block_dot(q["x"], q["u_s"], mask)
+    for q in st:
+        q["read"] = q["read"] - block_dot(q["corr_read"], q["pulled"], mask)
+        q["start"] = q["r_s"] - block_dot(q["corr_read"], q["reach"], mask)
+        c_hi, c_lo = halves(q["c_tail"])
+        k_hi, k_lo = halves(q["k_tail"])
+        rh, rl_ = halves(q["reach"])
+        full = (dot_dims(jnp.concatenate([rh, rl_, rh], axis=0),
+                         jnp.concatenate([c_hi, c_hi, c_lo], axis=0), TN))
+        q["map"] = jnp.where(same, jnp.where(diag, q["keep"], 0.0) - full, 0.0)
+        ph, pl_ = halves(-q["pulled"])
+        full = dot_dims(jnp.concatenate([q["val"], q["val"]], axis=0),
+                        jnp.concatenate([k_hi, k_lo], axis=0), TN)
+        full = full + dot_dims(jnp.concatenate([ph, pl_, ph], axis=0),
+                               jnp.concatenate([c_hi, c_hi, c_lo], axis=0), TN)
+        full = jnp.where(same, full, 0.0)
+        q["add"] = sum(full[g * CHUNK : (g + 1) * CHUNK] for g in range(1, width // CHUNK)) + full[:CHUNK]
+    ps = None
+    for c, q in enumerate(st):
+        rows = pl.ds(c * CHUNK, CHUNK)
+        if c == 0:
+            rd_ref[rows, :] = q["read"]
+            th_ref[rows, :] = q["start"]
+            m = q["map"]
+            p = sum(m[g * CHUNK : (g + 1) * CHUNK] for g in range(1, width // CHUNK)) + m[:CHUNK]
+            ps = jnp.concatenate([p, q["add"]], axis=0)
+        else:
+            th_ref[rows, :] = block_dot(q["start"], ps[:CHUNK], mask, NT)
+            rd_ref[rows, :] = q["read"] + block_dot(q["start"], ps[CHUNK:], mask, NT)
+            m_hi, m_lo = halves(q["map"])
+            ps = two_split(ps, m_hi, m_lo)
+            ps = jnp.concatenate([ps[:CHUNK], ps[CHUNK:] + q["add"]], axis=0)
+    ma_ref[...] = ps
+
+
+def mix_local(r, k, v, d, b):
+    t, w = r.shape
+    return pl.pallas_call(
+        mix_body,
+        out_shape=(
+            jax.ShapeDtypeStruct((t, w), F32),
+            jax.ShapeDtypeStruct((t, w), F32),
+            jax.ShapeDtypeStruct((2 * CHUNK, w), F32),
+        ),
+        in_specs=[pl.BlockSpec(memory_space=pltpu.VMEM)] * 5,
+        out_specs=(pl.BlockSpec(memory_space=pltpu.VMEM),) * 3,
+        compiler_params=pltpu.CompilerParams(vmem_limit_bytes=48 * 1024 * 1024),
+        name="mix_local",
+    )(r, k, v, d, b)
 
 
 def time_mix(
@@ -129,33 +246,13 @@
 ):
     tokens_here, channels = receptance.shape
     heads_here = channels // HEAD
-    block_shape = (tokens_here // SPAN, SPAN, heads_here, HEAD)
-
-    def arrange(array):
-        return array.astype(jnp.float32).reshape(block_shape)
-
-    recept = arrange(receptance)
-    keyvec = arrange(key_vectors)
-    valvec = arrange(value_vectors)
-    logdec = -jnp.exp(-jax.nn.softplus(-arrange(decay_logits)) - 0.5)
-    unit_key = keyvec / jnp.sqrt(1.0 + jnp.sum(keyvec * keyvec, axis=-1, keepdims=True))
-    correction = unit_key * jax.nn.sigmoid(arrange(rate_logits))
-    read_local, start_rows, block_map, block_add = block_pieces(
-        recept, keyvec, valvec, logdec, unit_key, correction
+    reads, through, ends = mix_local(
+        receptance, key_vectors, value_vectors, decay_logits, rate_logits
     )
     eye_heads = jnp.broadcast_to(jnp.eye(HEAD, dtype=jnp.float32), (heads_here, HEAD, HEAD))
     zero_heads = jnp.zeros((heads_here, HEAD, HEAD), jnp.float32)
-
-    def advance(carried, inputs):
-        local_state, product = carried
-        step_map, step_add = inputs
-        new_state = exact_einsum("hij,hjl->hil", local_state, step_map) + step_add
-        new_product = exact_einsum("hij,hjl->hil", product, step_map)
-        return ((new_state, new_product), (local_state, product))
-
-    (device_add, device_map), (starts, products) = lax.scan(
-        advance, (zero_heads, eye_heads), (block_map, block_add)
-    )
+    device_map = jnp.swapaxes(ends[:HEAD].reshape(HEAD, heads_here, HEAD), 0, 1)
+    device_add = jnp.swapaxes(ends[HEAD:].reshape(HEAD, heads_here, HEAD), 0, 1)
 
     def compose(earlier, following):
         return (
@@ -165,9 +262,10 @@
 
     prefix = carried_in((device_map, device_add), SP, compose, (eye_heads, zero_heads))
     incoming = prefix[1]
-    from_local = exact_einsum("bthj,bhij->bthi", start_rows, starts)
-    through = exact_einsum("bthl,bhjl->bthj", start_rows, products)
-    state_read = read_local + from_local + exact_einsum("bthj,hij->bthi", through, incoming)
+    head_shape = (tokens_here, heads_here, HEAD)
+    state_read = reads.reshape(head_shape) + exact_einsum(
+        "thj,hij->thi", through.reshape(head_shape), incoming
+    )
     centred = state_read - jnp.mean(state_read, axis=-1, keepdims=True)
     scaled = centred * lax.rsqrt(jnp.mean(centred * centred, axis=-1, keepdims=True) + EPS_GROUP)
     gated_out = (

time: 453 us -> 328 us (0.72)
  other arithmetic: 96.4 us -> 3.9 us
  matrix products: 46.5 us -> 15.2 us
  local copies, waits for them, and re-layouts: 30.4 us -> 23.4 us
  Pallas kernels: 0 us -> 4.98 us
    another operation x8 -> x3, other arithmetic: 82.5 us -> 1.21 us  [the longest x3 80.9 us: block_pieces(): jax.scipy.linalg.solve_triangular(system, jnp.concatenate([right_local, r...]
    dot_general x53 -> x24, matrix products: 39.1 us -> 8.94 us  [exact_einsum(): return jnp.einsum(pattern, first_op, second_op, precision=HIGHEST)]
    unnamed x79 -> x64, local copies, waits for them, and re-layouts: 1.9 us -> 9.5 us
    dynamic_update_slice x8 -> x0, local copies, waits for them, and re-layouts: 5.47 us -> none  [time_mix(): lax.scan(advance, (zero_heads, eye_heads), (block_map, block_add))]
    dynamic_update_slice x8 -> x0, other arithmetic: 5.32 us -> none  [time_mix(): lax.scan(advance, (zero_heads, eye_heads), (block_map, block_add))]
    pallas_call x0 -> x1, Pallas kernels: none -> 4.98 us  [mix_local(): pl.pallas_call(mix_body, out_shape=(jax.ShapeDtypeStruct((t, w), F32), ja...]
where the time goes in v1:
time: 328 us; the launch traced here: 327 us
  blocking collectives  206 us (63%)
  waiting for transfers between devices  55.2 us (17%)
  local copies, waits for them, and re-layouts  23.4 us (7%)
  starting transfers between devices  17.8 us (5%)
  matrix products  15.2 us (5%)
  Pallas kernels  4.98 us (2%)
  other arithmetic  3.9 us (1%)
    all_gather x4, blocking collectives, carried_in(): lax.all_gather(part.astype(kind), axis)  65.1 us
    all_to_all x1, blocking collectives, local(): lax.all_to_all(outgoing, SP, split_axis=0, concat_axis=0, tiled=True)  57.5 us
    all_to_all x1, blocking collectives, sent_and_summed(): pieces = lax.all_to_all(split_up(shard, dim, size), axis, 0, 0, tiled=True)  52.7 us
    all_to_all x1, waiting for transfers between devices, local(): lax.all_to_all(expert_res.astype(jnp.bfloat16).reshape(-1, capacity, feat...  33.4 us
    all_to_all x1, blocking collectives, from_everyone(): lax.all_to_all(jnp.broadcast_to(shard[None], (size, *shard.shape)), axis,...  30.5 us
    all_to_all x2, waiting for transfers between devices, from_everyone(): lax.all_to_all(jnp.broadcast_to(shard[None], (size, *shard.shape)), axis,...  21.9 us
    all_to_all x2, starting transfers between devices, from_everyone(): lax.all_to_all(jnp.broadcast_to(shard[None], (size, *shard.shape)), axis,...  10.6 us
    unnamed x64, local copies, waits for them, and re-layouts  9.5 us
  transfers between devices with their start and end apart: 3, of which 3 were waited for; matrix products, arithmetic and copies ran while one was open for 1% of the time, Pallas kernels for 0%

profile of v1, /device:TPU:1, one launch (start us, length us, event | category | flops | bytes accessed | tf_op | source)
XLA Modules:
  0.0 327.0 jit_solution(11656896259423426329)
XLA Ops:
  4.7 5.0 %mix_local.1 = (f32[256,256]{1,0:T(8,128)S(1)}, f32[256,256]{1,0:T(8,128)S(1)}, f32[128,256]{1,0:T(8,128)S(1)}) custom-call(bf16[256,256]{1,0:T(8,128)(2,1)S(1)} %copy-done.1, bf16[256,256]{1,0:T(8,128)(2,1)S(1)} %copy-done.2, bf16[256,256]{1,0:T(8,128)(2,1)S(1)} %copy-done.3, bf16[256,256]{1,0:T(8,128)(2,1)S(1)} %copy-done.4, bf16[256,256]{1,0:T(8,128)(2,1)S(1)} %copy-done.5), custom_call_target="tpu_custom_call" | custom-call | tf_op jit(solution)/shard_map/mix_local/pallas_call | solution.py:230
  9.8 8.4 %all-gather = bf16[8,64,64]{2,1,0:T(8,128)(2,1)S(1)} all-gather(bf16[4,64,64]{2,1,0:T(8,128)(2,1)S(1)} %bitcast.83), channel_id=2, replica_groups=mesh['sp_0'=16,'sp_1'=2,'tp'=16] {'sp_1'}, dimensions={0}, use_global_device_ids=true | all-gather | bytes 98304 | tf_op jit(solution)/shard_map/all_gather | solution.py:31
  18.4 1.9 all-gather.2
  21.3 29.5 %all-gather.3 = bf16[64,64,64]{2,1,0:T(8,128)(2,1)S(1)} all-gather(bf16[4,64,64]{2,1,0:T(8,128)(2,1)S(1)} %get-tuple-element.13), channel_id=5, replica_groups=mesh['sp_0'=16,'sp_1'=2,'tp'=16] {'sp_0'}, dimensions={0}, use_global_device_ids=true | all-gather | bytes 557056 | tf_op jit(solution)/shard_map/all_gather | solution.py:31
  51.9 25.3 %all-gather.1 = bf16[64,64,64]{2,1,0:T(8,128)(2,1)S(1)} all-gather(bf16[4,64,64]{2,1,0:T(8,128)(2,1)S(1)} %get-tuple-element.15), channel_id=3, replica_groups=mesh['sp_0'=16,'sp_1'=2,'tp'=16] {'sp_0'}, dimensions={0}, use_global_device_ids=true | all-gather | bytes 557056 | tf_op jit(solution)/shard_map/all_gather | solution.py:31
  87.1 1.1 fusion.11
  88.2 1.3 fusion.3
  91.0 1.5 broadcast_in_dim.22
  92.5 6.9 %all-to-all-start = ((bf16[16,256,256]{1,2,0:T(8,128)(2,1)}), bf16[16,256,256]{1,2,0:T(8,128)(2,1)}, u32[]{:S(2)}, u32[]{:S(2)}) async-start(bf16[16,256,256]{1,2,0:T(8,128)(2,1)} %broadcast_in_dim.22), calls=%async_computation | async-start | bytes 4194304 | tf_op jit(solution)/shard_map/all_to_all | solution.py:48
  99.9 1.2 reduce-window.6
  101.8 2.4 scatter_custom_fusion
  104.2 15.2 %all-to-all-done = bf16[16,256,256]{1,2,0:T(8,128)(2,1)} async-done(((bf16[16,256,256]{1,2,0:T(8,128)(2,1)}), bf16[16,256,256]{1,2,0:T(8,128)(2,1)}, u32[]{:S(2)}, u32[]{:S(2)}) %all-to-all-start) | async-done | bytes 2097184 | tf_op jit(solution)/shard_map/all_to_all | solution.py:48
  119.4 2.4 multiply_reduce_fusion.1
  122.5 3.7 %all-to-all-start.1 = ((f32[16,1,256]{2,1,0:T(1,128)}), f32[16,1,256]{2,1,0:T(1,128)S(1)}, u32[]{:S(2)}, u32[]{:S(2)}) async-start(f32[16,1,256]{2,1,0:T(1,128)} %broadcast_in_dim.23), calls=%async_computation.1 | async-start | bytes 32768 | tf_op jit(solution)/shard_map/all_to_all | solution.py:48
  126.2 6.7 %all-to-all-done.1 = f32[16,1,256]{2,1,0:T(1,128)S(1)} async-done(((f32[16,1,256]{2,1,0:T(1,128)}), f32[16,1,256]{2,1,0:T(1,128)S(1)}, u32[]{:S(2)}, u32[]{:S(2)}) %all-to-all-start.1) | async-done | bytes 16416 | tf_op jit(solution)/shard_map/all_to_all | solution.py:48
  133.0 3.9 %gather_fusion = bf16[1024,256]{1,0:T(8,128)(2,1)S(1)} fusion(bf16[257,256]{1,0:T(8,128)(2,1)S(1)} %concatenate.6, s32[1024]{0:T(1024)S(1)} %fusion.51), kind=kCustom, calls=%fused_computation | custom fusion | bytes 1052672 | tf_op jit(solution)/shard_map/gather | solution.py:322
  137.0 57.5 %all_to_all.31 = bf16[32,32,256]{2,1,0:T(8,128)(2,1)S(1)} all-to-all(bf16[32,32,256]{2,1,0:T(8,128)(2,1)S(1)} %bitcast.77), channel_id=1, replica_groups=mesh['sp_0'=16,'sp_1'=2,'tp'=16] {'sp_0','sp_1'}, dimensions={0} | all-to-all | bytes 1048576 | tf_op jit(solution)/shard_map/all_to_all | solution.py:323
  194.5 2.3 convolution_convert_fusion
  196.8 52.7 %all_to_all.32 = bf16[16,64,2048]{2,1,0:T(8,128)(2,1)S(1)} all-to-all(bf16[16,64,2048]{2,1,0:T(8,128)(2,1)S(1)} %bitcast.73), channel_id=1, replica_groups=mesh['sp_0'=16,'sp_1'=2,'tp'=16] {'tp'}, dimensions={0} | all-to-all | bytes 8388608 | tf_op jit(solution)/shard_map/all_to_all | solution.py:76
  250.6 30.5 %all_to_all.33 = bf16[16,64,1024]{2,1,0:T(8,128)(2,1)S(1)} all-to-all(bf16[16,64,1024]{2,1,0:T(8,128)(2,1)S(1)} %broadcast_in_dim.52), channel_id=1, replica_groups=mesh['sp_0'=16,'sp_1'=2,'tp'=16] {'tp'}, dimensions={0} | all-to-all | bytes 4194304 | tf_op jit(solution)/shard_map/all_to_all | solution.py:48
  281.1 1.5 convolution_convert_fusion.1
  282.6 7.2 %all-to-all-start.5 = ((bf16[32,32,256]{2,1,0:T(8,128)(2,1)}), bf16[32,32,256]{2,1,0:T(8,128)(2,1)S(1)}, u32[]{:S(2)}, u32[]{:S(2)}) async-start(bf16[32,32,256]{2,1,0:T(8,128)(2,1)} %bitcast.18), calls=%async_computation.5 | async-start | bytes 1048576 | tf_op jit(solution)/shard_map/all_to_all | solution.py:336
  290.0 33.4 %all-to-all-done.5 = bf16[32,32,256]{2,1,0:T(8,128)(2,1)S(1)} async-done(((bf16[32,32,256]{2,1,0:T(8,128)(2,1)}), bf16[32,32,256]{2,1,0:T(8,128)(2,1)S(1)}, u32[]{:S(2)}, u32[]{:S(2)}) %all-to-all-start.5) | async-done | bytes 524320 | tf_op jit(solution)/shard_map/all_to_all | solution.py:336
  323.4 1.9 gather_fusion.1
  (127 shorter events, 22.8 us)
Async XLA Ops:
  0.0 119.4 %copy-start = (bf16[4096,256]{1,0:T(8,128)(2,1)S(1)}, bf16[4096,256]{1,0:T(8,128)(2,1)}, u32[]{:S(2)}) copy-start(bf16[4096,256]{1,0:T(8,128)(2,1)} %param.23) | copy-start | bytes 6291460
  0.0 51.8 %copy-start.20 = (f32[64,64]{1,0:T(8,128)}, f32[64,64]{1,0:T(8,128)S(1)}, u32[]{:S(2)}) copy-start(f32[64,64]{1,0:T(8,128)S(1)} %fusion.50) | copy-start | bytes 49156
  0.0 1.1 copy-start.1
  1.1 0.9 copy-start.2
  2.0 0.9 copy-start.3
  50.8 33.1 %copy-start.6 = (bf16[64,64,64]{2,1,0:T(8,128)(2,1)}, bf16[64,64,64]{2,1,0:T(8,128)(2,1)S(1)}, u32[]{:S(2)}) copy-start(bf16[64,64,64]{2,1,0:T(8,128)(2,1)S(1)} %all-gather.3) | copy-start | bytes 1572868
  77.2 6.8 %copy-start.7 = (bf16[64,64,64]{2,1,0:T(8,128)(2,1)}, bf16[64,64,64]{2,1,0:T(8,128)(2,1)S(1)}, u32[]{:S(2)}) copy-start(bf16[64,64,64]{2,1,0:T(8,128)(2,1)S(1)} %all-gather.1) | copy-start | bytes 1572868
  77.4 1.0 copy-start.17
  86.3 3.5 %copy-start.16 = (f32[4,64,64]{2,1,0:T(8,128)S(1)}, f32[4,64,64]{2,1,0:T(8,128)}, u32[]{:S(2)}) copy-start(f32[4,64,64]{2,1,0:T(8,128)} %copy-done.15) | copy-start | bytes 196612
  86.3 3.5 %copy-start.21 = (f32[64,64]{1,0:T(8,128)S(1)}, f32[64,64]{1,0:T(8,128)}, u32[]{:S(2)}) copy-start(f32[64,64]{1,0:T(8,128)} %copy-done.20) | copy-start | bytes 49156
  87.1 2.7 copy-start.22
  87.1 3.0 copy-start.18
  87.1 3.0 copy-start.19
  89.5 1.2 copy-start.24
  89.5 1.2 copy-start.27
  92.5 6.9 %copy-start.25 = (s32[256,2]{0,1:T(2,128)S(1)}, s32[256,2]{0,1:T(2,128)}, u32[]{:S(2)}) copy-start(s32[256,2]{0,1:T(2,128)} %param.25) | copy-start | bytes 6148
  92.5 26.9 %copy-start.30 = (bf16[256,256]{1,0:T(8,128)(2,1)S(1)}, bf16[256,256]{1,0:T(8,128)(2,1)}, u32[]{:S(2)}) copy-start(bf16[256,256]{1,0:T(8,128)(2,1)} %param.22) | copy-start | bytes 393220
  92.5 26.9 %all-to-all-start = ((bf16[16,256,256]{1,2,0:T(8,128)(2,1)}), bf16[16,256,256]{1,2,0:T(8,128)(2,1)}, u32[]{:S(2)}, u32[]{:S(2)}) async-start(bf16[16,256,256]{1,2,0:T(8,128)(2,1)} %broadcast_in_dim.22), calls=%async_computation | async-start | bytes 4194304 | tf_op jit(solution)/shard_map/all_to_all | solution.py:48
  119.4 13.5 %copy-start.28 = (f32[256]{0:T(256)S(1)}, f32[256]{0:T(256)}, u32[]{:S(2)}) copy-start(f32[256]{0:T(256)} %param.24) | copy-start | bytes 3076
  122.5 10.4 %all-to-all-start.1 = ((f32[16,1,256]{2,1,0:T(1,128)}), f32[16,1,256]{2,1,0:T(1,128)S(1)}, u32[]{:S(2)}, u32[]{:S(2)}) async-start(f32[16,1,256]{2,1,0:T(1,128)} %broadcast_in_dim.23), calls=%async_computation.1 | async-start | bytes 32768 | tf_op jit(solution)/shard_map/all_to_all | solution.py:48
  133.0 61.4 %copy-start.23 = (bf16[1,256,1024]{2,1,0:T(8,128)(2,1)S(1)}, bf16[1,256,1024]{2,1,0:T(8,128)(2,1)}, u32[]{:S(2)}) copy-start(bf16[1,256,1024]{2,1,0:T(8,128)(2,1)} %param.28) | copy-start | bytes 1572868
  250.6 30.5 %copy-start.29 = (bf16[1,1024,256]{2,1,0:T(8,128)(2,1)S(1)}, bf16[1,1024,256]{2,1,0:T(8,128)(2,1)}, u32[]{:S(2)}) copy-start(bf16[1,1024,256]{2,1,0:T(8,128)(2,1)} %param.29) | copy-start | bytes 1572868
  281.1 8.7 %copy-start.26 = (f32[256,2]{0,1:T(2,128)S(1)}, f32[256,2]{0,1:T(2,128)}, u32[]{:S(2)}) copy-start(f32[256,2]{0,1:T(2,128)} %param.26) | copy-start | bytes 6148
  282.6 40.8 %all-to-all-start.5 = ((bf16[32,32,256]{2,1,0:T(8,128)(2,1)}), bf16[32,32,256]{2,1,0:T(8,128)(2,1)S(1)}, u32[]{:S(2)}, u32[]{:S(2)}) async-start(bf16[32,32,256]{2,1,0:T(8,128)(2,1)} %bitcast.18), calls=%async_computation.5 | async-start | bytes 1048576 | tf_op jit(solution)/shard_map/all_to_all | solution.py:336
  (10 other events, 7.2 us)

commit v2 on v1

--- a/solution.py
+++ b/solution.py
@@ -1,3 +1,4 @@
+import functools
 import jax
 import jax.numpy as jnp
 from jax import lax
@@ -8,39 +9,12 @@
 
 D = 4096
 HEAD = 64
-SP = ("sp_0", "sp_1")
+SP = ("z", "c")
+TP = ("y", "x")
 
 
 EPS_GROUP = 0.00064
 EPS_NORM = 1e-06
-HIGHEST = lax.Precision.HIGHEST
-
-
-def neutral_like(shard, identity):
-    return jax.tree.map(
-        lambda part, zero: jnp.zeros_like(part) + jnp.asarray(zero, part.dtype), shard, identity
-    )
-
-
-def carried_in(shard, axes, combine, identity):
-    before = start = neutral_like(shard, identity)
-    so_far = shard
-    for axis in reversed(axes):
-        size, mine = (lax.axis_size(axis), lax.axis_index(axis))
-        pieces = jax.tree.map(
-            lambda part, kind: lax.all_gather(part.astype(kind), axis),
-            so_far,
-            (jnp.bfloat16, jnp.bfloat16),
-        )
-        inside, so_far = (start, start)
-        for k in range(size):
-            passed = k < mine
-            so_far = combine(
-                so_far, jax.tree.map(lambda part, own: part[k].astype(own.dtype), pieces, shard)
-            )
-            inside = jax.tree.map(lambda new, old: jnp.where(passed, new, old), so_far, inside)
-        before = combine(inside, before)
-    return before
 
 
 def from_everyone(shard, axis):
@@ -75,10 +49,6 @@
     size = lax.axis_size(axis)
     pieces = lax.all_to_all(split_up(shard, dim, size), axis, 0, 0, tiled=True)
     return jnp.sum(pieces.astype(jnp.float32), axis=0)
-
-
-def exact_einsum(pattern, first_op, second_op):
-    return jnp.einsum(pattern, first_op, second_op, precision=HIGHEST)
 
 
 F32 = jnp.float32
@@ -241,39 +211,245 @@
     )(r, k, v, d, b)
 
 
-def time_mix(
-    receptance, key_vectors, value_vectors, decay_logits, rate_logits, gate_logits, group_gain
-):
-    tokens_here, channels = receptance.shape
-    heads_here = channels // HEAD
-    reads, through, ends = mix_local(
-        receptance, key_vectors, value_vectors, decay_logits, rate_logits
-    )
-    eye_heads = jnp.broadcast_to(jnp.eye(HEAD, dtype=jnp.float32), (heads_here, HEAD, HEAD))
-    zero_heads = jnp.zeros((heads_here, HEAD, HEAD), jnp.float32)
-    device_map = jnp.swapaxes(ends[:HEAD].reshape(HEAD, heads_here, HEAD), 0, 1)
-    device_add = jnp.swapaxes(ends[HEAD:].reshape(HEAD, heads_here, HEAD), 0, 1)
-
-    def compose(earlier, following):
-        return (
-            exact_einsum("hij,hjl->hil", earlier[0], following[0]),
-            exact_einsum("hij,hjl->hil", earlier[1], following[0]) + following[1],
-        )
-
-    prefix = carried_in((device_map, device_add), SP, compose, (eye_heads, zero_heads))
-    incoming = prefix[1]
-    head_shape = (tokens_here, heads_here, HEAD)
-    state_read = reads.reshape(head_shape) + exact_einsum(
-        "thj,hij->thi", through.reshape(head_shape), incoming
-    )
-    centred = state_read - jnp.mean(state_read, axis=-1, keepdims=True)
-    scaled = centred * lax.rsqrt(jnp.mean(centred * centred, axis=-1, keepdims=True) + EPS_GROUP)
-    gated_out = (
-        scaled.reshape(tokens_here, channels)
-        * group_gain[None, :]
-        * jax.nn.sigmoid(gate_logits.astype(jnp.float32))
-    )
-    return gated_out.astype(jnp.bfloat16)
+MESH = pl.DeviceIdType.MESH
+
+
+def ring_order(size):
+    near = sorted(range(1, size), key=lambda k: (min(k, size - k), k))
+    return near
+
+
+def remote(src, dst, send, recv, **where):
+    return pltpu.make_async_remote_copy(
+        src_ref=src, dst_ref=dst, send_sem=send, recv_sem=recv, device_id=where, device_id_type=MESH
+    )
+
+
+def greet(targets):
+    barrier = pltpu.get_barrier_semaphore()
+    for where in targets:
+        pl.semaphore_signal(barrier, inc=1, device_id=where, device_id_type=MESH)
+    pl.semaphore_wait(barrier, len(targets))
+
+
+def share_blocks(buf, send, recv, y, x, ny, nx, use):
+    mine = y * nx + x
+    half = buf.shape[1] // 2
+    sent = []
+
+    def view(slot, part):
+        return buf.at[slot, pl.ds(part * half, half), :]
+
+    def push(slot, part, **where):
+        copy = remote(view(slot, part), view(slot, part), send.at[len(sent)], recv.at[part, slot], **where)
+        copy.start()
+        sent.append(copy)
+
+    def arrived(slot, part):
+        remote(view(slot, part), view(slot, part), send.at[0], recv.at[part, slot], x=x).wait_recv()
+
+    xs, ys = ring_order(nx), ring_order(ny)
+    for k in range(max(len(xs), len(ys))):
+        if k < len(xs):
+            push(mine, 0, x=lax.rem(x + xs[k], nx))
+        if k < len(ys):
+            push(mine, 1, y=lax.rem(y + ys[k], ny))
+    for k in ys:
+        push(mine, 0, y=lax.rem(y + k, ny))
+    for k in xs:
+        push(mine, 1, x=lax.rem(x + k, nx))
+    use(mine, 0)
+    use(mine, 1)
+    for k in range(max(len(xs), len(ys))):
+        if k < len(xs):
+            slot = y * nx + lax.rem(x + nx - xs[k], nx)
+            arrived(slot, 0)
+            for j in ys:
+                push(slot, 0, y=lax.rem(y + j, ny))
+            use(slot, 0)
+        if k < len(ys):
+            slot = lax.rem(y + ny - ys[k], ny) * nx + x
+            arrived(slot, 1)
+            for j in xs:
+                push(slot, 1, x=lax.rem(x + j, nx))
+            use(slot, 1)
+    for k in ys:
+        slot = lax.rem(y + ny - k, ny) * nx + x
+        arrived(slot, 0)
+        use(slot, 0)
+    for k in xs:
+        slot = y * nx + lax.rem(x + nx - k, nx)
+        arrived(slot, 1)
+        use(slot, 1)
+    for a in xs:
+        for b in ys:
+            for part, (j, k) in ((0, (b, a)), (1, (b, a))):
+                slot = lax.rem(y + ny - j, ny) * nx + lax.rem(x + nx - k, nx)
+                arrived(slot, part)
+                use(slot, part)
+    return sent
+
+
+def exact_left(a, b, mask, dims=NN):
+    b_hi, b_lo = halves(b)
+    return dot_dims(a, block_diag(b_hi, mask), dims) + dot_dims(a, block_diag(b_lo, mask), dims)
+
+
+def flow_body(nz, ny, nx, rd_ref, th_ref, ma_ref, gate_ref, gain_ref, res_ref, ngain_ref, w_ref,
+              mid_ref, norm_ref,
+              pair_out, pair_in, hop_out, hop_in, near_in, far_out, far_in, back_out, back_in,
+              blocks, total, sq_out, sq_in,
+              pair_s, hop_s, fin_s, back_s, ag_send, ag_recv, sq_send, sq_recv):
+    z, c, y, x = (lax.axis_index(name) for name in ("z", "c", "y", "x"))
+    steps = []
+    d = 1
+    while d < nz // 2:
+        steps.append(d)
+        d *= 2
+    far = nz // 2 + 1
+    xs, ys = ring_order(nx), ring_order(ny)
+    who = [dict(c=1 - c)]
+    offs = []
+    for d in steps + [1, far]:
+        for o in (d, nz - d):
+            if o % nz and o not in offs:
+                offs.append(o)
+    who += [dict(z=lax.rem(z + o, nz)) for o in offs]
+    plane = [(a, b) for a in range(ny) for b in range(nx) if (a, b) != (0, 0)]
+    who += [dict(y=lax.rem(y + a, ny), x=lax.rem(x + b, nx)) for a, b in plane]
+    greet(who)
+
+    wide = ma_ref.shape[1]
+    part = wide // 2
+    ends = ma_ref[...]
+    low, high = ends[:, :part], ends[:, part:]
+    first = c == 0
+    pair_out[...] = jnp.where(first, high, low).astype(BF16)
+    swap = remote(pair_out, pair_in, pair_s.at[0], pair_s.at[1], c=1 - c)
+    swap.start()
+    mine = jnp.where(first, low, high)
+    mask = ((iota2((part, part), 0) // CHUNK) == (iota2((part, part), 1) // CHUNK)).astype(F32).astype(BF16)
+    swap.wait()
+    peer = pair_in[...].astype(F32)
+    early = jnp.where(first, mine, peer)
+    late = jnp.where(first, peer, mine)
+
+    def compose(before, after):
+        moved = block_dot(before, after[:CHUNK], mask)
+        return jnp.concatenate([moved[:CHUNK], moved[CHUNK:] + after[CHUNK:]], axis=0)
+
+    cur = compose(early, late)
+    for i, d in enumerate(steps):
+        hop_out[i] = cur.astype(BF16)
+        hop = remote(hop_out.at[i], hop_in.at[i], hop_s.at[0, i], hop_s.at[1, i], z=lax.rem(z + d, nz))
+        hop.start()
+        hop.wait()
+        joined = compose(hop_in[i].astype(F32), cur)
+        cur = jnp.where(z >= d, joined, cur)
+    last = len(steps)
+    hop_out[last] = cur.astype(BF16)
+    far_out[...] = cur[CHUNK:].astype(BF16)
+    far_copy = remote(far_out, far_in, fin_s.at[0], fin_s.at[1], z=lax.rem(z + far, nz))
+    far_copy.start()
+    near_copy = remote(hop_out.at[last], near_in, fin_s.at[2], fin_s.at[3], z=lax.rem(z + 1, nz))
+    near_copy.start()
+    near_copy.wait()
+    near = jnp.where(z >= 1, near_in[...].astype(F32), 0.0)
+    far_copy.wait()
+    far_add = jnp.where(z >= far, far_in[...].astype(F32), 0.0)
+    start0 = block_dot(far_add, near[:CHUNK], mask) + near[CHUNK:]
+    start1 = block_dot(start0, early[:CHUNK], mask) + early[CHUNK:]
+    own = jnp.where(first, start0, start1)
+    back_out[...] = jnp.where(first, start1, start0).astype(BF16)
+    back = remote(back_out, back_in, back_s.at[0], back_s.at[1], c=1 - c)
+    back.start()
+    back.wait()
+    other = back_in[...].astype(F32)
+    incoming = jnp.concatenate([jnp.where(first, own, other), jnp.where(first, other, own)], axis=1)
+
+    mask4 = ((iota2((wide, wide), 0) // CHUNK) == (iota2((wide, wide), 1) // CHUNK)).astype(F32).astype(BF16)
+    read = rd_ref[...] + block_dot(th_ref[...], incoming, mask4, NT)
+    centred = read - left_split(read, mask4) * (1.0 / CHUNK)
+    spread = left_split(centred * centred, mask4) * (1.0 / CHUNK)
+    gate = 1.0 / (1.0 + jnp.exp(-gate_ref[...].astype(F32)))
+    mixed = centred * lax.rsqrt(spread + EPS_GROUP) * gain_ref[...] * gate
+    tp = y * nx + x
+    blocks[tp] = mixed.astype(BF16)
+    total[...] = res_ref[...].astype(F32)
+    half = blocks.shape[1] // 2
+
+    def project(slot, part_no):
+        rows = pl.ds(part_no * half, half)
+        total[rows, :] += jnp.dot(blocks[slot, rows, :], w_ref[slot], preferred_element_type=F32)
+
+    sent = share_blocks(blocks, ag_send, ag_recv, y, x, ny, nx, project)
+    midway = total[...].astype(BF16)
+    mid_ref[...] = midway
+    mid_f = midway.astype(F32)
+    s_hi, s_lo = halves(mid_f * mid_f)
+    ones = jnp.ones((8, wide), BF16)
+    sums = dot_dims(ones, s_hi, NT) + dot_dims(ones, s_lo, NT)
+    sq_out[...] = sums
+    pieces = []
+    for i, (a, b) in enumerate(plane):
+        copy = remote(sq_out, sq_in.at[i], sq_send.at[i], sq_recv.at[i],
+                      y=lax.rem(y + a, ny), x=lax.rem(x + b, nx))
+        copy.start()
+        pieces.append(copy)
+    for i, copy in enumerate(pieces):
+        copy.wait_recv()
+        sums = sums + sq_in[i]
+    t_hi, t_lo = halves(sums)
+    t_mid, t_lo = halves(sums - t_hi.astype(F32))
+    eighth = jnp.full((8, wide), 0.125, BF16)
+    squares = dot_dims(t_hi, eighth, TN) + dot_dims(t_mid, eighth, TN) + dot_dims(t_lo, eighth, TN)
+    inv = lax.rsqrt(squares * (1.0 / (wide * ny * nx)) + EPS_NORM)
+    norm_ref[...] = (mid_f * ngain_ref[...] * inv).astype(BF16)
+    for copy in sent + pieces:
+        copy.wait_send()
+
+
+def flow(sizes, rd, th, ma, gate, gain, res, ngain, w):
+    nz, ny, nx = sizes
+    rows, wide = rd.shape
+    part = wide // 2
+    tp = ny * nx
+    nstep = max(nz.bit_length() - 2, 0)
+    dma = pltpu.SemaphoreType.DMA
+    vm = pl.BlockSpec(memory_space=pltpu.VMEM)
+    return pl.pallas_call(
+        functools.partial(flow_body, nz, ny, nx),
+        out_shape=(jax.ShapeDtypeStruct((rows, wide), BF16),) * 2,
+        in_specs=[vm] * 8,
+        out_specs=(vm, vm),
+        scratch_shapes=[
+            pltpu.VMEM((2 * CHUNK, part), BF16),
+            pltpu.VMEM((2 * CHUNK, part), BF16),
+            pltpu.VMEM((nstep + 1, 2 * CHUNK, part), BF16),
+            pltpu.VMEM((max(nstep, 1), 2 * CHUNK, part), BF16),
+            pltpu.VMEM((2 * CHUNK, part), BF16),
+            pltpu.VMEM((CHUNK, part), BF16),
+            pltpu.VMEM((CHUNK, part), BF16),
+            pltpu.VMEM((CHUNK, part), BF16),
+            pltpu.VMEM((CHUNK, part), BF16),
+            pltpu.VMEM((tp, rows, wide), BF16),
+            pltpu.VMEM((rows, wide), F32),
+            pltpu.VMEM((8, rows), F32),
+            pltpu.VMEM((tp - 1, 8, rows), F32),
+            dma((2,)),
+            dma((2, max(nstep, 1))),
+            dma((4,)),
+            dma((2,)),
+            dma((2 * (tp - 1),)),
+            dma((2, tp)),
+            dma((tp - 1,)),
+            dma((tp - 1,)),
+        ],
+        compiler_params=pltpu.CompilerParams(
+            collective_id=0, has_side_effects=True, vmem_limit_bytes=32 * 1024 * 1024
+        ),
+        name="flow",
+    )(rd, th, ma, gate, gain, res, ngain, w)
 
 
 def local(
@@ -293,18 +469,17 @@
     expert_up,
     expert_down,
 ):
-    mixed_rows = time_mix(
-        receptance, key_vectors, value_vectors, decay_logits, rate_logits, gate_logits, group_gain
+    reads, through, ends = mix_local(
+        receptance, key_vectors, value_vectors, decay_logits, rate_logits
     )
     tokens_here, features = residual.shape
-    projected = jnp.dot(
-        gather_directly(mixed_rows, "tp", 1), mixer_out, preferred_element_type=jnp.float32
-    )
-    midway = (residual.astype(jnp.float32) + projected).astype(jnp.bfloat16)
+    sizes = tuple(lax.axis_size(name) for name in ("z", "y", "x"))
+    planes = sizes[1] * sizes[2]
+    midway, normed = flow(
+        sizes, reads, through, ends, gate_logits, group_gain[None], residual, norm_gain[None],
+        mixer_out.reshape(planes, -1, features),
+    )
     midway_f = midway.astype(jnp.float32)
-    squares = of_everyone(jnp.sum(midway_f * midway_f, axis=1), "tp")
-    inv_rms = lax.rsqrt(squares / D + EPS_NORM)
-    normed = (midway_f * norm_gain[None, :] * inv_rms[:, None]).astype(jnp.bfloat16)
     routes = expert_ids.shape[1]
     experts_all = lax.axis_size(SP) * expert_gate.shape[0]
     capacity = 2 * tokens_here * routes // experts_all
@@ -325,13 +500,13 @@
     paired = jnp.concatenate([expert_gate[0], expert_up[0]], axis=1)
     gate_up = sent_and_summed(
         jnp.dot(arrived_rows, paired, preferred_element_type=jnp.float32).astype(jnp.bfloat16),
-        "tp",
+        TP,
         0,
     )
     half_width = paired.shape[1] // 2
     hidden = (jax.nn.silu(gate_up[:, :half_width]) * gate_up[:, half_width:]).astype(jnp.bfloat16)
     expert_res = jnp.dot(
-        gather_directly(hidden, "tp", 0), expert_down[0], preferred_element_type=jnp.float32
+        gather_directly(hidden, TP, 0), expert_down[0], preferred_element_type=jnp.float32
     )
     returned = lax.all_to_all(
         expert_res.astype(jnp.bfloat16).reshape(-1, capacity, features),
@@ -350,27 +525,27 @@
 
 
 def solution(mesh):
-    torus = Mesh(mesh.devices.reshape(16, 2, mesh.shape["tp"]), ("sp_0", "sp_1", "tp"))
+    torus = Mesh(mesh.devices.reshape(16, 2, 4, 4), ("z", "c", "y", "x"))
     return jax.shard_map(
         local,
         mesh=torus,
         in_specs=(
-            P(SP, "tp"),
-            P(SP, "tp"),
-            P(SP, "tp"),
-            P(SP, "tp"),
-            P(SP, "tp"),
-            P(SP, "tp"),
-            P("tp"),
-            P(SP, "tp"),
-            P(None, "tp"),
-            P("tp"),
+            P(SP, TP),
+            P(SP, TP),
+            P(SP, TP),
+            P(SP, TP),
+            P(SP, TP),
+            P(SP, TP),
+            P(TP),
+            P(SP, TP),
+            P(None, TP),
+            P(TP),
             P(SP, None),
             P(SP, None),
-            P(SP, "tp", None),
-            P(SP, "tp", None),
-            P(SP, None, "tp"),
+            P(SP, TP, None),
+            P(SP, TP, None),
+            P(SP, None, TP),
         ),
-        out_specs=P(SP, "tp"),
+        out_specs=P(SP, TP),
         check_vma=False,
     )

time: 328 us -> 261 us (0.80)
  blocking collectives: 206 us -> 126 us
  Pallas kernels: 4.98 us -> 67.1 us
  waiting for transfers between devices: 55.2 us -> 33.4 us
  matrix products: 15.2 us -> 2.75 us
  starting transfers between devices: 17.8 us -> 7.24 us
  local copies, waits for them, and re-layouts: 23.4 us -> 19.9 us
    all_gather x4 -> x0, blocking collectives: 65.1 us -> none  [carried_in(): lax.all_gather(part.astype(kind), axis)]
    pallas_call x0 -> x1, Pallas kernels: none -> 62.2 us  [flow(): pl.pallas_call(functools.partial(flow_body, nz, ny, nx), out_shape=(jax.S...]
    all_to_all x2 -> x0, waiting for transfers between devices: 21.9 us -> none  [from_everyone(): lax.all_to_all(jnp.broadcast_to(shard[None], (size, *shard.shape)), axis,...]
    all_to_all x1, blocking collectives: 57.5 us -> 41 us  [local(): lax.all_to_all(outgoing, SP, split_axis=0, concat_axis=0, tiled=True)]
    dot_general x26 -> x1, matrix products: 12.9 us -> 1.5 us  [local(): jnp.dot(gather_directly(hidden, TP, 0), expert_down[0], preferred_element...]
    all_to_all x2 -> x0, starting transfers between devices: 10.6 us -> none  [from_everyone(): lax.all_to_all(jnp.broadcast_to(shard[None], (size, *shard.shape)), axis,...]
    unnamed x64 -> x30, local copies, waits for them, and re-layouts: 9.5 us -> 10.3 us
  transfers between devices with their start and end apart: 3 -> 1, of which waited for: 3 -> 1; matrix products, arithmetic and copies ran while one was open for 1% -> 0% of each run, Pallas kernels for 0% -> 0%
where the time goes in v2:
time: 261 us
  blocking collectives  126 us (48%)
  Pallas kernels  67.1 us (26%)
  waiting for transfers between devices  33.4 us (13%)
  local copies, waits for them, and re-layouts  19.9 us (8%)
  starting transfers between devices  7.24 us (3%)
  other arithmetic  4.26 us (2%)
  matrix products  2.75 us (1%)
    pallas_call x1, Pallas kernels, flow(): pl.pallas_call(functools.partial(flow_body, nz, ny, nx), out_shape=(jax.S...  62.2 us
    all_to_all x1, blocking collectives, sent_and_summed(): pieces = lax.all_to_all(split_up(shard, dim, size), axis, 0, 0, tiled=True)  54.5 us
    all_to_all x1, blocking collectives, local(): lax.all_to_all(outgoing, SP, split_axis=0, concat_axis=0, tiled=True)  41 us
    all_to_all x1, waiting for transfers between devices, local(): lax.all_to_all(expert_res.astype(jnp.bfloat16).reshape(-1, capacity, feat...  33.4 us
    all_to_all x1, blocking collectives, from_everyone(): lax.all_to_all(jnp.broadcast_to(shard[None], (size, *shard.shape)), axis,...  30.4 us
    unnamed x30, local copies, waits for them, and re-layouts  10.3 us
    all_to_all x1, starting transfers between devices, local(): lax.all_to_all(expert_res.astype(jnp.bfloat16).reshape(-1, capacity, feat...  7.24 us
  transfers between devices with their start and end apart: 1, of which 1 were waited for; matrix products, arithmetic and copies ran while one was open for 0% of the time, Pallas kernels for 0%

profile of v2, /device:TPU:1, one launch (start us, length us, event | category | flops | bytes accessed | tf_op | source)
XLA Modules:
  0.0 260.8 jit_solution(3033030977811698604)
XLA Ops:
  0.0 0.9 copy.18
  1.9 1.2 reduce-window.6
  3.7 2.4 scatter_custom_fusion
  6.2 0.9 copy-done.2
  7.1 0.9 copy-done.3
  8.0 0.9 copy-done.4
  8.9 0.9 copy-done.5
  9.8 0.9 copy-done.6
  10.7 5.0 %mix_local.1 = (f32[256,256]{1,0:T(8,128)S(1)}, f32[256,256]{1,0:T(8,128)S(1)}, f32[128,256]{1,0:T(8,128)S(1)}) custom-call(bf16[256,256]{1,0:T(8,128)(2,1)S(1)} %copy-done.2, bf16[256,256]{1,0:T(8,128)(2,1)S(1)} %copy-done.3, bf16[256,256]{1,0:T(8,128)(2,1)S(1)} %copy-done.4, bf16[256,256]{1,0:T(8,128)(2,1)S(1)} %copy-done.5, bf16[256,256]{1,0:T(8,128)(2,1)S(1)} %copy-done.6), custom_call_target="tpu_custom_call" | custom-call | tf_op jit(solution)/shard_map/mix_local/pallas_call | solution.py:200
  15.7 1.6 copy-done.1
  17.3 0.9 copy-done.7
  18.2 0.9 copy-done.8
  20.4 62.2 %flow.1 = (bf16[256,256]{1,0:T(8,128)(2,1)S(1)}, bf16[256,256]{1,0:T(8,128)(2,1)S(1)}) custom-call(f32[256,256]{1,0:T(8,128)S(1)} %get-tuple-element.10.rd_ref, f32[256,256]{1,0:T(8,128)S(1)} %get-tuple-element.11.th_ref, f32[128,256]{1,0:T(8,128)S(1)} %get-tuple-element.12.ma_ref, bf16[256,256]{1,0:T(8,128)(2,1)S(1)} %copy-done.7, f32[1,256]{1,0:T(1,128)S(1)} %bitcast.38, ...), custom_call_target="tpu_custom_call" | custom-call | tf_op jit(solution)/shard_map/flow/pallas_call | solution.py:420
  82.7 3.9 %gather_fusion = bf16[1024,256]{1,0:T(8,128)(2,1)S(1)} fusion(bf16[257,256]{1,0:T(8,128)(2,1)S(1)} %concatenate.6, s32[1024]{0:T(1024)S(1)} %fusion.9), kind=kCustom, calls=%fused_computation | custom fusion | bytes 1052672 | tf_op jit(solution)/shard_map/gather | solution.py:497
  86.6 41.0 %all_to_all.20 = bf16[32,32,256]{2,1,0:T(8,128)(2,1)S(1)} all-to-all(bf16[32,32,256]{2,1,0:T(8,128)(2,1)S(1)} %bitcast.44), channel_id=1, replica_groups=mesh['z'=16,'c'=2,'y'=4,'x'=4] {'z','c'}, dimensions={0} | all-to-all | bytes 1048576 | tf_op jit(solution)/shard_map/all_to_all | solution.py:498
  127.7 1.3 convolution_convert_fusion
  128.9 54.5 %all_to_all.21 = bf16[16,64,2048]{2,1,0:T(8,128)(2,1)S(1)} all-to-all(bf16[16,64,2048]{2,1,0:T(8,128)(2,1)S(1)} %bitcast.40), channel_id=1, replica_groups=mesh['z'=16,'c'=2,'y'=4,'x'=4] {'y','x'}, dimensions={0} | all-to-all | bytes 8388608 | tf_op jit(solution)/shard_map/all_to_all | solution.py:50
  183.4 0.8 convert_reduce_fusion
  184.5 30.4 %all_to_all.22 = bf16[16,64,1024]{2,1,0:T(8,128)(2,1)S(1)} all-to-all(bf16[16,64,1024]{2,1,0:T(8,128)(2,1)S(1)} %broadcast_in_dim.27), channel_id=1, replica_groups=mesh['z'=16,'c'=2,'y'=4,'x'=4] {'y','x'}, dimensions={0} | all-to-all | bytes 4194304 | tf_op jit(solution)/shard_map/all_to_all | solution.py:22
  214.9 1.5 convolution_convert_fusion.1
  216.4 7.2 %all-to-all-start.3 = ((bf16[32,32,256]{2,1,0:T(8,128)(2,1)}), bf16[32,32,256]{2,1,0:T(8,128)(2,1)S(1)}, u32[]{:S(2)}, u32[]{:S(2)}) async-start(bf16[32,32,256]{2,1,0:T(8,128)(2,1)} %bitcast.13), calls=%async_computation.3 | async-start | bytes 1048576 | tf_op jit(solution)/shard_map/all_to_all | solution.py:511
  223.8 33.4 %all-to-all-done.3 = bf16[32,32,256]{2,1,0:T(8,128)(2,1)S(1)} async-done(((bf16[32,32,256]{2,1,0:T(8,128)(2,1)}), bf16[32,32,256]{2,1,0:T(8,128)(2,1)S(1)}, u32[]{:S(2)}, u32[]{:S(2)}) %all-to-all-start.3) | async-done | bytes 524320 | tf_op jit(solution)/shard_map/all_to_all | solution.py:511
  257.2 1.9 gather_fusion.1
  259.4 0.7 multiply_reduce_fusion
  (40 shorter events, 4.5 us)
Async XLA Ops:
  0.0 214.9 %copy-start = (bf16[1,1024,256]{2,1,0:T(8,128)(2,1)S(1)}, bf16[1,1024,256]{2,1,0:T(8,128)(2,1)}, u32[]{:S(2)}) copy-start(bf16[1,1024,256]{2,1,0:T(8,128)(2,1)} %param.29) | copy-start | bytes 1572868
  6.2 0.9 copy-start.2
  7.1 0.9 copy-start.3
  8.0 0.9 copy-start.4
  8.9 0.9 copy-start.5
  9.8 0.9 copy-start.6
  15.7 1.6 copy-start.1
  17.3 0.9 copy-start.7
  18.2 0.9 copy-start.8
  19.1 0.7 copy-start.9
  19.8 0.7 copy-start.10
  82.6 45.0 %copy-start.11 = (bf16[1,256,1024]{2,1,0:T(8,128)(2,1)S(1)}, bf16[1,256,1024]{2,1,0:T(8,128)(2,1)}, u32[]{:S(2)}) copy-start(bf16[1,256,1024]{2,1,0:T(8,128)(2,1)} %param.28) | copy-start | bytes 1572868
  82.7 45.0 %copy-start.12 = (bf16[1,256,1024]{2,1,0:T(8,128)(2,1)S(1)}, bf16[1,256,1024]{2,1,0:T(8,128)(2,1)}, u32[]{:S(2)}) copy-start(bf16[1,256,1024]{2,1,0:T(8,128)(2,1)} %param.27) | copy-start | bytes 1572868
  214.9 8.8 %copy-start.13 = (f32[256,2]{0,1:T(2,128)S(1)}, f32[256,2]{0,1:T(2,128)}, u32[]{:S(2)}) copy-start(f32[256,2]{0,1:T(2,128)} %param.26) | copy-start | bytes 6148
  216.4 40.8 %all-to-all-start.3 = ((bf16[32,32,256]{2,1,0:T(8,128)(2,1)}), bf16[32,32,256]{2,1,0:T(8,128)(2,1)S(1)}, u32[]{:S(2)}, u32[]{:S(2)}) async-start(bf16[32,32,256]{2,1,0:T(8,128)(2,1)} %bitcast.13), calls=%async_computation.3 | async-start | bytes 1048576 | tf_op jit(solution)/shard_map/all_to_all | solution.py:511

commit v3 on v2

--- a/solution.py
+++ b/solution.py
@@ -7,48 +7,12 @@
 from jax.sharding import Mesh
 from jax.sharding import PartitionSpec as P
 
-D = 4096
-HEAD = 64
 SP = ("z", "c")
 TP = ("y", "x")
 
 
 EPS_GROUP = 0.00064
 EPS_NORM = 1e-06
-
-
-def from_everyone(shard, axis):
-    size = lax.axis_size(axis)
-    return lax.all_to_all(
-        jnp.broadcast_to(shard[None], (size, *shard.shape)), axis, 0, 0, tiled=True
-    )
-
-
-def joined_along(pieces, dim):
-    dims = list(pieces.shape[1:])
-    dims[dim] *= pieces.shape[0]
-    return jnp.moveaxis(pieces, 0, dim).reshape(dims)
-
-
-def gather_directly(shard, axis, dim):
-    pieces = from_everyone(shard, axis)
-    return joined_along(pieces, dim)
-
-
-def of_everyone(shard, axis):
-    everything = from_everyone(shard, axis)
-    return jnp.sum(everything, axis=0)
-
-
-def split_up(shard, dim, size):
-    before, after = (shard.shape[:dim], shard.shape[dim + 1 :])
-    return jnp.moveaxis(shard.reshape(*before, size, -1, *after), dim, 0)
-
-
-def sent_and_summed(shard, axis, dim):
-    size = lax.axis_size(axis)
-    pieces = lax.all_to_all(split_up(shard, dim, size), axis, 0, 0, tiled=True)
-    return jnp.sum(pieces.astype(jnp.float32), axis=0)
 
 
 F32 = jnp.float32
@@ -452,6 +416,257 @@
     )(rd, th, ma, gate, gain, res, ngain, w)
 
 
+def experts_body(nz, ny, nx, norm_ref, mid_ref, ids_ref, rw_ref, wg_ref, wu_ref, wd_ref, out_ref,
+                 going, came, parts, from_x, from_y, sum_a, sum_b, last_a, last_b, hid, res, back,
+                 pick_hi, pick_lo,
+                 go_s, go_r, x_s, x_r, y_s, y_r, a_s, a_r, b_s, b_r, ag_send, ag_recv, re_s, re_r):
+    z, c, y, x = (lax.axis_index(name) for name in ("z", "c", "y", "x"))
+    me = 2 * z + c
+    tp = y * nx + x
+    tokens = norm_ref.shape[0]
+    count, cap, _ = going.shape
+    slots = count * cap
+    ff = wg_ref.shape[1]
+    hf = ff // 2
+    xs, ys = ring_order(nx), ring_order(ny)
+    zs = ring_order(nz)
+
+    def core_of(flip):
+        return 1 - c if flip else c
+
+    barrier = pltpu.get_barrier_semaphore()
+    who = [dict(c=1 - c)]
+    who += [dict(z=lax.rem(z + o, nz), c=core_of(f)) for o in zs for f in (0, 1)]
+    who += [dict(x=lax.rem(x + k, nx)) for k in xs] + [dict(y=lax.rem(y + k, ny)) for k in ys]
+    for where in who:
+        pl.semaphore_signal(barrier, inc=1, device_id=where, device_id_type=MESH)
+
+    ids = ids_ref[...]
+    id0, id1 = ids[:, 0:1], ids[:, 1:2]
+    lane = iota2((tokens, 128), 1)
+    hit = jnp.where((lane == id0) | (lane == id1), 1.0, 0.0).astype(BF16)
+    tri = jnp.where(iota2((tokens, tokens), 1) < iota2((tokens, tokens), 0), 1.0, 0.0).astype(BF16)
+    earlier = dot_dims(tri, hit, NN)
+
+    def slot_of(one):
+        rank = jnp.sum(jnp.where(lane == one, earlier, 0.0), axis=1, keepdims=True)
+        return one * cap + rank.astype(jnp.int32)
+
+    slot0, slot1 = slot_of(id0), slot_of(id1)
+    spot = iota2((tokens, slots), 1)
+    hot0, hot1 = spot == slot0, spot == slot1
+    take = jnp.where(hot0 | hot1, 1.0, 0.0).astype(BF16)
+    going[...] = dot_dims(take, norm_ref[...], TN).astype(BF16).reshape(going.shape)
+    pl.semaphore_wait(barrier, len(who))
+
+    sent = []
+
+    def dispatch(zt, ct):
+        e = 2 * zt + ct
+        copy = remote(going.at[e], came.at[me], go_s.at[len(sent)], go_r.at[me], z=zt, c=ct)
+        copy.start()
+        sent.append(copy)
+
+    came[me] = going[me]
+    dispatch(z, 1 - c)
+    for o in zs:
+        for f in (0, 1):
+            dispatch(lax.rem(z + o, nz), core_of(f))
+    rw = rw_ref[...]
+    weight = jnp.where(hot0, rw[:, 0:1], 0.0) + jnp.where(hot1, rw[:, 1:2], 0.0)
+    w_hi, w_lo = halves(weight)
+    pick_hi[...] = w_hi
+    pick_lo[...] = w_lo
+
+    def take_in(src):
+        @pl.when(src != me)
+        def _():
+            remote(came.at[src], came.at[src], go_s.at[0], go_r.at[src], c=1 - c).wait_recv()
+
+    def to_x(t):
+        xt, yt = lax.rem(t, nx), lax.div(t, nx)
+        return remote(parts.at[t, 0], from_x.at[x, yt], x_s.at[t], x_r.at[x, yt], x=xt)
+
+    def to_y(t):
+        xt, yt = lax.rem(t, nx), lax.div(t, nx)
+        return remote(parts.at[t, 1], from_y.at[y, xt], y_s.at[t], y_r.at[y, xt], y=yt)
+
+    def gate_up(k, carry):
+        off = jnp.where(lax.rem(k, 2) == 1, lax.div(k + 1, 2), nz - lax.div(k, 2))
+        t = lax.rem(z + off, nz)
+        take_in(2 * t)
+        take_in(2 * t + 1)
+        rows = came[pl.ds(2 * t, 2)].reshape(2 * cap, came.shape[2])
+        gate = jnp.dot(rows, wg_ref[...], preferred_element_type=F32).astype(BF16)
+        up = jnp.dot(rows, wu_ref[...], preferred_element_type=F32).astype(BF16)
+        parts[t, 0, :, :hf] = gate[:, :hf]
+        parts[t, 0, :, hf:] = up[:, :hf]
+        parts[t, 1, :, :hf] = gate[:, hf:]
+        parts[t, 1, :, hf:] = up[:, hf:]
+
+        @pl.when(lax.rem(t, nx) != x)
+        def _():
+            to_x(t).start()
+
+        @pl.when(lax.div(t, nx) != y)
+        def _():
+            to_y(t).start()
+
+        return carry
+
+    lax.fori_loop(0, nz, gate_up, 0)
+
+    def added_a(yb):
+        acc = parts[yb * nx + x, 0].astype(F32)
+        for k in xs:
+            src = lax.rem(x + nx - k, nx)
+            remote(from_x.at[src, yb], from_x.at[src, yb], x_s.at[0], x_r.at[src, yb], x=src).wait_recv()
+            acc = acc + from_x[src, yb].astype(F32)
+        return acc
+
+    def added_b(xb):
+        acc = parts[y * nx + xb, 1].astype(F32)
+        for k in ys:
+            src = lax.rem(y + ny - k, ny)
+            remote(from_y.at[src, xb], from_y.at[src, xb], y_s.at[0], y_r.at[src, xb], y=src).wait_recv()
+            acc = acc + from_y[src, xb].astype(F32)
+        return acc
+
+    second = []
+    for k in range(max(len(xs), len(ys))):
+        if k < len(ys):
+            yb = lax.rem(y + ys[k], ny)
+            sum_a[k] = added_a(yb).astype(BF16)
+            copy = remote(sum_a.at[k], last_a.at[k], a_s.at[k], a_r.at[k], y=yb)
+            copy.start()
+            second.append(copy)
+        if k < len(xs):
+            xb = lax.rem(x + xs[k], nx)
+            sum_b[k] = added_b(xb).astype(BF16)
+            copy = remote(sum_b.at[k], last_b.at[k], b_s.at[k], b_r.at[k], x=xb)
+            copy.start()
+            second.append(copy)
+    tot_a = added_a(y)
+    tot_b = added_b(x)
+    for copy in second:
+        copy.wait_recv()
+    for k in range(len(ys)):
+        tot_a = tot_a + last_a[k].astype(F32)
+    for k in range(len(xs)):
+        tot_b = tot_b + last_b[k].astype(F32)
+
+    def act(both):
+        gate, up = both[:, :hf], both[:, hf:]
+        return (gate / (1.0 + jnp.exp(-gate)) * up).astype(BF16)
+
+    hid[tp, :, :hf] = act(tot_a)
+    hid[tp, :, hf:] = act(tot_b)
+
+    def give_back(slot, part):
+        return remote(res.at[slot, part], back.at[me], re_s.at[slot, part], re_r.at[me], z=slot, c=part)
+
+    def down(slot, part):
+        rows = hid[slot, pl.ds(part * cap, cap), :]
+        value = jnp.dot(rows, wd_ref[...], preferred_element_type=F32).astype(BF16)
+        res[slot, part] = value
+        own = jnp.logical_and(slot == z, c == part)
+
+        @pl.when(own)
+        def _():
+            back[me] = value
+
+        @pl.when(jnp.logical_not(own))
+        def _():
+            give_back(slot, part).start()
+
+    shared = share_blocks(hid, ag_send, ag_recv, y, x, ny, nx, down)
+
+    def collect(src, carry):
+        @pl.when(src != me)
+        def _():
+            remote(back.at[src], back.at[src], re_s.at[0, 0], re_r.at[src], c=1 - c).wait_recv()
+
+        return carry
+
+    lax.fori_loop(0, count, collect, 0)
+    rows = back[...].reshape(slots, back.shape[2])
+    routed = dot_dims(pick_hi[...], rows, NN) + dot_dims(pick_lo[...], rows, NN)
+    out_ref[...] = (mid_ref[...].astype(F32) + routed).astype(BF16)
+
+    for copy in sent + second + shared:
+        copy.wait_send()
+
+    def drain(t, carry):
+        @pl.when(lax.rem(t, nx) != x)
+        def _():
+            to_x(t).wait_send()
+
+        @pl.when(lax.div(t, nx) != y)
+        def _():
+            to_y(t).wait_send()
+
+        for part in (0, 1):
+            @pl.when(jnp.logical_not(jnp.logical_and(t == z, c == part)))
+            def _():
+                give_back(t, part).wait_send()
+
+        return carry
+
+    lax.fori_loop(0, nz, drain, 0)
+
+
+def experts(sizes, normed, midway, ids, weights, wg, wu, wd):
+    nz, ny, nx = sizes
+    tokens, wide = normed.shape
+    ff = wg.shape[1]
+    count = 2 * nz
+    cap = 2 * tokens * ids.shape[1] // count
+    tp = ny * nx
+    rows = 2 * cap
+    dma = pltpu.SemaphoreType.DMA
+    vm = pl.BlockSpec(memory_space=pltpu.VMEM)
+    return pl.pallas_call(
+        functools.partial(experts_body, nz, ny, nx),
+        out_shape=jax.ShapeDtypeStruct((tokens, wide), BF16),
+        in_specs=[vm] * 7,
+        out_specs=vm,
+        scratch_shapes=[
+            pltpu.VMEM((count, cap, wide), BF16),
+            pltpu.VMEM((count, cap, wide), BF16),
+            pltpu.VMEM((nz, 2, rows, ff), BF16),
+            pltpu.VMEM((nx, ny, rows, ff), BF16),
+            pltpu.VMEM((ny, nx, rows, ff), BF16),
+            pltpu.VMEM((ny - 1, rows, ff), BF16),
+            pltpu.VMEM((nx - 1, rows, ff), BF16),
+            pltpu.VMEM((ny - 1, rows, ff), BF16),
+            pltpu.VMEM((nx - 1, rows, ff), BF16),
+            pltpu.VMEM((tp, rows, ff), BF16),
+            pltpu.VMEM((nz, 2, cap, wide), BF16),
+            pltpu.VMEM((count, cap, wide), BF16),
+            pltpu.VMEM((tokens, count * cap), BF16),
+            pltpu.VMEM((tokens, count * cap), BF16),
+            dma((count - 1,)),
+            dma((count,)),
+            dma((nz,)),
+            dma((nx, ny)),
+            dma((nz,)),
+            dma((ny, nx)),
+            dma((ny - 1,)),
+            dma((ny - 1,)),
+            dma((nx - 1,)),
+            dma((nx - 1,)),
+            dma((2 * (tp - 1),)),
+            dma((2, tp)),
+            dma((nz, 2)),
+            dma((count,)),
+        ],
+        compiler_params=pltpu.CompilerParams(
+            collective_id=1, has_side_effects=True, vmem_limit_bytes=48 * 1024 * 1024
+        ),
+        name="experts",
+    )(normed, midway, ids, weights, wg, wu, wd)
+
+
 def local(
     receptance,
     key_vectors,
@@ -479,49 +694,10 @@
         sizes, reads, through, ends, gate_logits, group_gain[None], residual, norm_gain[None],
         mixer_out.reshape(planes, -1, features),
     )
-    midway_f = midway.astype(jnp.float32)
-    routes = expert_ids.shape[1]
-    experts_all = lax.axis_size(SP) * expert_gate.shape[0]
-    capacity = 2 * tokens_here * routes // experts_all
-    flat_ids = expert_ids.reshape(-1)
-    onehot = (flat_ids[:, None] == jnp.arange(experts_all, dtype=jnp.int32)[None, :]).astype(
-        jnp.int32
+    return experts(
+        sizes, normed, midway, expert_ids, route_weight,
+        expert_gate[0], expert_up[0], expert_down[0],
     )
-    earlier_count = jnp.sum((jnp.cumsum(onehot, axis=0) - onehot) * onehot, axis=1)
-    slot_of = flat_ids * capacity + earlier_count
-    owner_token = jnp.arange(tokens_here * routes, dtype=jnp.int32) // routes
-    slot_table = (
-        jnp.full((experts_all * capacity,), tokens_here, jnp.int32).at[slot_of].set(owner_token)
-    )
-    padded = jnp.concatenate([normed, jnp.zeros((1, features), jnp.bfloat16)], axis=0)
-    outgoing = padded[slot_table].reshape(experts_all, capacity, features)
-    arrived = lax.all_to_all(outgoing, SP, split_axis=0, concat_axis=0, tiled=True)
-    arrived_rows = arrived.reshape(-1, features)
-    paired = jnp.concatenate([expert_gate[0], expert_up[0]], axis=1)
-    gate_up = sent_and_summed(
-        jnp.dot(arrived_rows, paired, preferred_element_type=jnp.float32).astype(jnp.bfloat16),
-        TP,
-        0,
-    )
-    half_width = paired.shape[1] // 2
-    hidden = (jax.nn.silu(gate_up[:, :half_width]) * gate_up[:, half_width:]).astype(jnp.bfloat16)
-    expert_res = jnp.dot(
-        gather_directly(hidden, TP, 0), expert_down[0], preferred_element_type=jnp.float32
-    )
-    returned = lax.all_to_all(
-        expert_res.astype(jnp.bfloat16).reshape(-1, capacity, features),
-        SP,
-        split_axis=0,
-        concat_axis=0,
-        tiled=True,
-    )
-    picked = (
-        returned.reshape(-1, features)[slot_of]
-        .astype(jnp.float32)
-        .reshape(tokens_here, routes, features)
-    )
-    routed_sum = jnp.sum(picked * route_weight[:, :, None], axis=1)
-    return (midway_f + routed_sum).astype(jnp.bfloat16)
 
 
 def solution(mesh):

time: 261 us -> 175 us (0.67)
  the two profiles are of different devices: /device:TPU:1 before, /device:TPU:21 now
where the time goes in v3:
time: 175 us
  Pallas kernels  164 us (94%)
  local copies, waits for them, and re-layouts  10.3 us (6%)
    pallas_call x1, Pallas kernels, experts(): pl.pallas_call(functools.partial(experts_body, nz, ny, nx), out_shape=jax...  100 us
    pallas_call x1, Pallas kernels, flow(): pl.pallas_call(functools.partial(flow_body, nz, ny, nx), out_shape=(jax.S...  58.9 us
    unnamed x33, local copies, waits for them, and re-layouts  10.3 us
    pallas_call x1, Pallas kernels, mix_local(): pl.pallas_call(mix_body, out_shape=(jax.ShapeDtypeStruct((t, w), F32), ja...  4.97 us

profile of v3, /device:TPU:21, one launch (start us, length us, event | category | flops | bytes accessed | tf_op | source)
XLA Modules:
  0.0 174.8 jit_solution(15108046255100264205)
XLA Ops:
  0.0 0.0 copy-start.1
  0.0 0.0 copy-start.4
  0.0 1.0 copy-done.4
  1.0 0.9 copy-done.5
  1.9 0.9 copy-done.6
  2.8 0.9 copy-done.7
  3.7 0.9 copy-done.8
  4.6 5.0 %mix_local.1 = (f32[256,256]{1,0:T(8,128)S(1)}, f32[256,256]{1,0:T(8,128)S(1)}, f32[128,256]{1,0:T(8,128)S(1)}) custom-call(bf16[256,256]{1,0:T(8,128)(2,1)S(1)} %copy-done.4, bf16[256,256]{1,0:T(8,128)(2,1)S(1)} %copy-done.5, bf16[256,256]{1,0:T(8,128)(2,1)S(1)} %copy-done.6, bf16[256,256]{1,0:T(8,128)(2,1)S(1)} %copy-done.7, bf16[256,256]{1,0:T(8,128)(2,1)S(1)} %copy-done.8), custom_call_target="tpu_custom_call" | custom-call | tf_op jit(solution)/shard_map/mix_local/pallas_call | solution.py:164
  9.6 0.0 copy-start
  9.6 1.6 copy-done
  11.2 0.9 copy-done.9
  12.1 0.9 copy-done.10
  13.0 0.7 copy-done.11
  13.7 0.7 copy-done.12
  14.3 58.9 %flow.1 = (bf16[256,256]{1,0:T(8,128)(2,1)S(1)}, bf16[256,256]{1,0:T(8,128)(2,1)S(1)}) custom-call(f32[256,256]{1,0:T(8,128)S(1)} %get-tuple-element.10.rd_ref, f32[256,256]{1,0:T(8,128)S(1)} %get-tuple-element.11.th_ref, f32[128,256]{1,0:T(8,128)S(1)} %get-tuple-element.12.ma_ref, bf16[256,256]{1,0:T(8,128)(2,1)S(1)} %copy-done.9, f32[1,256]{1,0:T(1,128)S(1)} %bitcast.10, ...), custom_call_target="tpu_custom_call" | custom-call | tf_op jit(solution)/shard_map/flow/pallas_call | solution.py:384
  73.3 0.0 copy-done.13
  73.3 0.1 copy.16.ids_ref
  73.4 0.0 copy-done.14
  73.5 0.1 copy.17.rw_ref
  73.6 0.0 copy-done.1
  73.6 0.0 copy-done.2
  73.6 0.0 copy-done.3
  73.6 100.5 %experts.1 = bf16[256,256]{1,0:T(8,128)(2,1)S(1)} custom-call(bf16[256,256]{1,0:T(8,128)(2,1)S(1)} %get-tuple-element.13.norm_ref, bf16[256,256]{1,0:T(8,128)(2,1)S(1)} %get-tuple-element.14.mid_ref, s32[256,2]{1,0:T(8,128)S(1)} %copy.16.ids_ref, f32[256,2]{1,0:T(8,128)S(1)} %copy.17.rw_ref, bf16[256,1024]{1,0:T(8,128)(2,1)S(1)} %bitcast.7, ...), custom_call_target="tpu_custom_call" | custom-call | tf_op jit(solution)/shard_map/experts/pallas_call | solution.py:628
  174.1 0.7 copy.19
  (12 shorter events, 0.0 us)
Async XLA Ops:
  0.0 73.6 %copy-start.1 = (bf16[1,256,1024]{2,1,0:T(8,128)(2,1)S(1)}, bf16[1,256,1024]{2,1,0:T(8,128)(2,1)}, u32[]{:S(2)}) copy-start(bf16[1,256,1024]{2,1,0:T(8,128)(2,1)} %param.27) | copy-start | bytes 1572868
  0.0 1.0 copy-start.4
  1.0 0.9 copy-start.5
  1.9 0.9 copy-start.6
  2.8 0.9 copy-start.7
  3.7 0.9 copy-start.8
  4.6 68.7 %copy-start.13 = (s32[256,2]{0,1:T(2,128)S(1)}, s32[256,2]{0,1:T(2,128)}, u32[]{:S(2)}) copy-start(s32[256,2]{0,1:T(2,128)} %param.25) | copy-start | bytes 6148
  4.6 68.9 %copy-start.14 = (f32[256,2]{0,1:T(2,128)S(1)}, f32[256,2]{0,1:T(2,128)}, u32[]{:S(2)}) copy-start(f32[256,2]{0,1:T(2,128)} %param.26) | copy-start | bytes 6148
  9.6 1.6 copy-start
  11.2 0.9 copy-start.9
  12.1 0.9 copy-start.10
  13.0 0.7 copy-start.11
  13.7 0.7 copy-start.12
  14.3 59.3 %copy-start.2 = (bf16[1,256,1024]{2,1,0:T(8,128)(2,1)S(1)}, bf16[1,256,1024]{2,1,0:T(8,128)(2,1)}, u32[]{:S(2)}) copy-start(bf16[1,256,1024]{2,1,0:T(8,128)(2,1)} %param.28) | copy-start | bytes 1572868
  14.3 59.3 %copy-start.3 = (bf16[1,1024,256]{2,1,0:T(8,128)(2,1)S(1)}, bf16[1,1024,256]{2,1,0:T(8,128)(2,1)}, u32[]{:S(2)}) copy-start(bf16[1,1024,256]{2,1,0:T(8,128)(2,1)} %param.29) | copy-start | bytes 1572868

commit v4 on v3

--- a/solution.py
+++ b/solution.py
@@ -9,12 +9,6 @@
 
 SP = ("z", "c")
 TP = ("y", "x")
-
-
-EPS_GROUP = 0.00064
-EPS_NORM = 1e-06
-
-
 F32 = jnp.float32
 BF16 = jnp.bfloat16
 CHUNK = 64
@@ -159,23 +153,9 @@
     ma_ref[...] = ps
 
 
-def mix_local(r, k, v, d, b):
-    t, w = r.shape
-    return pl.pallas_call(
-        mix_body,
-        out_shape=(
-            jax.ShapeDtypeStruct((t, w), F32),
-            jax.ShapeDtypeStruct((t, w), F32),
-            jax.ShapeDtypeStruct((2 * CHUNK, w), F32),
-        ),
-        in_specs=[pl.BlockSpec(memory_space=pltpu.VMEM)] * 5,
-        out_specs=(pl.BlockSpec(memory_space=pltpu.VMEM),) * 3,
-        compiler_params=pltpu.CompilerParams(vmem_limit_bytes=48 * 1024 * 1024),
-        name="mix_local",
-    )(r, k, v, d, b)
-
-
 MESH = pl.DeviceIdType.MESH
+EPS_GROUP = 0.00064
+EPS_NORM = 1e-06
 
 
 def ring_order(size):
@@ -187,13 +167,6 @@
     return pltpu.make_async_remote_copy(
         src_ref=src, dst_ref=dst, send_sem=send, recv_sem=recv, device_id=where, device_id_type=MESH
     )
-
-
-def greet(targets):
-    barrier = pltpu.get_barrier_semaphore()
-    for where in targets:
-        pl.semaphore_signal(barrier, inc=1, device_id=where, device_id_type=MESH)
-    pl.semaphore_wait(barrier, len(targets))
 
 
 def share_blocks(buf, send, recv, y, x, ny, nx, use):
@@ -272,17 +245,7 @@
         d *= 2
     far = nz // 2 + 1
     xs, ys = ring_order(nx), ring_order(ny)
-    who = [dict(c=1 - c)]
-    offs = []
-    for d in steps + [1, far]:
-        for o in (d, nz - d):
-            if o % nz and o not in offs:
-                offs.append(o)
-    who += [dict(z=lax.rem(z + o, nz)) for o in offs]
     plane = [(a, b) for a in range(ny) for b in range(nx) if (a, b) != (0, 0)]
-    who += [dict(y=lax.rem(y + a, ny), x=lax.rem(x + b, nx)) for a, b in plane]
-    greet(who)
-
     wide = ma_ref.shape[1]
     part = wide // 2
     ends = ma_ref[...]
@@ -293,7 +256,8 @@
     swap.start()
     mine = jnp.where(first, low, high)
     mask = ((iota2((part, part), 0) // CHUNK) == (iota2((part, part), 1) // CHUNK)).astype(F32).astype(BF16)
-    swap.wait()
+    with jax.named_scope("pair"):
+        swap.wait()
     peer = pair_in[...].astype(F32)
     early = jnp.where(first, mine, peer)
     late = jnp.where(first, peer, mine)
@@ -307,7 +271,8 @@
         hop_out[i] = cur.astype(BF16)
         hop = remote(hop_out.at[i], hop_in.at[i], hop_s.at[0, i], hop_s.at[1, i], z=lax.rem(z + d, nz))
         hop.start()
-        hop.wait()
+        with jax.named_scope(f"hop{d}"):
+            hop.wait()
         joined = compose(hop_in[i].astype(F32), cur)
         cur = jnp.where(z >= d, joined, cur)
     last = len(steps)
@@ -317,9 +282,11 @@
     far_copy.start()
     near_copy = remote(hop_out.at[last], near_in, fin_s.at[2], fin_s.at[3], z=lax.rem(z + 1, nz))
     near_copy.start()
-    near_copy.wait()
+    with jax.named_scope("near"):
+        near_copy.wait()
     near = jnp.where(z >= 1, near_in[...].astype(F32), 0.0)
-    far_copy.wait()
+    with jax.named_scope("far"):
+        far_copy.wait()
     far_add = jnp.where(z >= far, far_in[...].astype(F32), 0.0)
     start0 = block_dot(far_add, near[:CHUNK], mask) + near[CHUNK:]
     start1 = block_dot(start0, early[:CHUNK], mask) + early[CHUNK:]
@@ -327,7 +294,8 @@
     back_out[...] = jnp.where(first, start1, start0).astype(BF16)
     back = remote(back_out, back_in, back_s.at[0], back_s.at[1], c=1 - c)
     back.start()
-    back.wait()
+    with jax.named_scope("back"):
+        back.wait()
     other = back_in[...].astype(F32)
     incoming = jnp.concatenate([jnp.where(first, own, other), jnp.where(first, other, own)], axis=1)
 
@@ -346,7 +314,8 @@
         rows = pl.ds(part_no * half, half)
         total[rows, :] += jnp.dot(blocks[slot, rows, :], w_ref[slot], preferred_element_type=F32)
 
-    sent = share_blocks(blocks, ag_send, ag_recv, y, x, ny, nx, project)
+    with jax.named_scope("share"):
+        sent = share_blocks(blocks, ag_send, ag_recv, y, x, ny, nx, project)
     midway = total[...].astype(BF16)
     mid_ref[...] = midway
     mid_f = midway.astype(F32)
@@ -360,9 +329,10 @@
                       y=lax.rem(y + a, ny), x=lax.rem(x + b, nx))
         copy.start()
         pieces.append(copy)
-    for i, copy in enumerate(pieces):
-        copy.wait_recv()
-        sums = sums + sq_in[i]
+    with jax.named_scope("squares"):
+        for i, copy in enumerate(pieces):
+            copy.wait_recv()
+            sums = sums + sq_in[i]
     t_hi, t_lo = halves(sums)
     t_mid, t_lo = halves(sums - t_hi.astype(F32))
     eighth = jnp.full((8, wide), 0.125, BF16)
@@ -371,49 +341,6 @@
     norm_ref[...] = (mid_f * ngain_ref[...] * inv).astype(BF16)
     for copy in sent + pieces:
         copy.wait_send()
-
-
-def flow(sizes, rd, th, ma, gate, gain, res, ngain, w):
-    nz, ny, nx = sizes
-    rows, wide = rd.shape
-    part = wide // 2
-    tp = ny * nx
-    nstep = max(nz.bit_length() - 2, 0)
-    dma = pltpu.SemaphoreType.DMA
-    vm = pl.BlockSpec(memory_space=pltpu.VMEM)
-    return pl.pallas_call(
-        functools.partial(flow_body, nz, ny, nx),
-        out_shape=(jax.ShapeDtypeStruct((rows, wide), BF16),) * 2,
-        in_specs=[vm] * 8,
-        out_specs=(vm, vm),
-        scratch_shapes=[
-            pltpu.VMEM((2 * CHUNK, part), BF16),
-            pltpu.VMEM((2 * CHUNK, part), BF16),
-            pltpu.VMEM((nstep + 1, 2 * CHUNK, part), BF16),
-            pltpu.VMEM((max(nstep, 1), 2 * CHUNK, part), BF16),
-            pltpu.VMEM((2 * CHUNK, part), BF16),
-            pltpu.VMEM((CHUNK, part), BF16),
-            pltpu.VMEM((CHUNK, part), BF16),
-            pltpu.VMEM((CHUNK, part), BF16),
-            pltpu.VMEM((CHUNK, part), BF16),
-            pltpu.VMEM((tp, rows, wide), BF16),
-            pltpu.VMEM((rows, wide), F32),
-            pltpu.VMEM((8, rows), F32),
-            pltpu.VMEM((tp - 1, 8, rows), F32),
-            dma((2,)),
-            dma((2, max(nstep, 1))),
-            dma((4,)),
-            dma((2,)),
-            dma((2 * (tp - 1),)),
-            dma((2, tp)),
-            dma((tp - 1,)),
-            dma((tp - 1,)),
-        ],
-        compiler_params=pltpu.CompilerParams(
-            collective_id=0, has_side_effects=True, vmem_limit_bytes=32 * 1024 * 1024
-        ),
-        name="flow",
-    )(rd, th, ma, gate, gain, res, ngain, w)
 
 
 def experts_body(nz, ny, nx, norm_ref, mid_ref, ids_ref, rw_ref, wg_ref, wu_ref, wd_ref, out_ref,
@@ -434,13 +361,6 @@
     def core_of(flip):
         return 1 - c if flip else c
 
-    barrier = pltpu.get_barrier_semaphore()
-    who = [dict(c=1 - c)]
-    who += [dict(z=lax.rem(z + o, nz), c=core_of(f)) for o in zs for f in (0, 1)]
-    who += [dict(x=lax.rem(x + k, nx)) for k in xs] + [dict(y=lax.rem(y + k, ny)) for k in ys]
-    for where in who:
-        pl.semaphore_signal(barrier, inc=1, device_id=where, device_id_type=MESH)
-
     ids = ids_ref[...]
     id0, id1 = ids[:, 0:1], ids[:, 1:2]
     lane = iota2((tokens, 128), 1)
@@ -452,12 +372,12 @@
         rank = jnp.sum(jnp.where(lane == one, earlier, 0.0), axis=1, keepdims=True)
         return one * cap + rank.astype(jnp.int32)
 
-    slot0, slot1 = slot_of(id0), slot_of(id1)
+    with jax.named_scope("route"):
+        slot0, slot1 = slot_of(id0), slot_of(id1)
     spot = iota2((tokens, slots), 1)
     hot0, hot1 = spot == slot0, spot == slot1
     take = jnp.where(hot0 | hot1, 1.0, 0.0).astype(BF16)
     going[...] = dot_dims(take, norm_ref[...], TN).astype(BF16).reshape(going.shape)
-    pl.semaphore_wait(barrier, len(who))
 
     sent = []
 
@@ -514,7 +434,8 @@
 
         return carry
 
-    lax.fori_loop(0, nz, gate_up, 0)
+    with jax.named_scope("gateup"):
+        lax.fori_loop(0, nz, gate_up, 0)
 
     def added_a(yb):
         acc = parts[yb * nx + x, 0].astype(F32)
@@ -533,23 +454,25 @@
         return acc
 
     second = []
-    for k in range(max(len(xs), len(ys))):
-        if k < len(ys):
-            yb = lax.rem(y + ys[k], ny)
-            sum_a[k] = added_a(yb).astype(BF16)
-            copy = remote(sum_a.at[k], last_a.at[k], a_s.at[k], a_r.at[k], y=yb)
-            copy.start()
-            second.append(copy)
-        if k < len(xs):
-            xb = lax.rem(x + xs[k], nx)
-            sum_b[k] = added_b(xb).astype(BF16)
-            copy = remote(sum_b.at[k], last_b.at[k], b_s.at[k], b_r.at[k], x=xb)
-            copy.start()
-            second.append(copy)
+    with jax.named_scope("second"):
+        for k in range(max(len(xs), len(ys))):
+            if k < len(ys):
+                yb = lax.rem(y + ys[k], ny)
+                sum_a[k] = added_a(yb).astype(BF16)
+                copy = remote(sum_a.at[k], last_a.at[k], a_s.at[k], a_r.at[k], y=yb)
+                copy.start()
+                second.append(copy)
+            if k < len(xs):
+                xb = lax.rem(x + xs[k], nx)
+                sum_b[k] = added_b(xb).astype(BF16)
+                copy = remote(sum_b.at[k], last_b.at[k], b_s.at[k], b_r.at[k], x=xb)
+                copy.start()
+                second.append(copy)
     tot_a = added_a(y)
     tot_b = added_b(x)
-    for copy in second:
-        copy.wait_recv()
+    with jax.named_scope("last"):
+        for copy in second:
+            copy.wait_recv()
     for k in range(len(ys)):
         tot_a = tot_a + last_a[k].astype(F32)
     for k in range(len(xs)):
@@ -579,7 +502,8 @@
         def _():
             give_back(slot, part).start()
 
-    shared = share_blocks(hid, ag_send, ag_recv, y, x, ny, nx, down)
+    with jax.named_scope("down"):
+        shared = share_blocks(hid, ag_send, ag_recv, y, x, ny, nx, down)
 
     def collect(src, carry):
         @pl.when(src != me)
@@ -588,7 +512,8 @@
 
         return carry
 
-    lax.fori_loop(0, count, collect, 0)
+    with jax.named_scope("collect"):
+        lax.fori_loop(0, count, collect, 0)
     rows = back[...].reshape(slots, back.shape[2])
     routed = dot_dims(pick_hi[...], rows, NN) + dot_dims(pick_lo[...], rows, NN)
     out_ref[...] = (mid_ref[...].astype(F32) + routed).astype(BF16)
@@ -612,59 +537,140 @@
 
         return carry
 
-    lax.fori_loop(0, nz, drain, 0)
-
-
-def experts(sizes, normed, midway, ids, weights, wg, wu, wd):
+    with jax.named_scope("drain"):
+        lax.fori_loop(0, nz, drain, 0)
+
+def layer_body(nz, ny, nx, r_hbm, k_hbm, v_hbm, d_hbm, b_hbm, gate_hbm, gain_ref, res_hbm, w_hbm, ngain_ref,
+               ids_ref, rw_ref, wg_hbm, wu_hbm, wd_hbm, out_ref,
+               r_ref, k_ref, v_ref, d_ref, b_ref, gate_ref, res_ref, w_ref, wg_ref, wu_ref, wd_ref,
+               rd_ref, th_ref, ma_ref, mid_ref, norm_ref, load_s, *rest):
+    z, c, y, x = (lax.axis_index(name) for name in ("z", "c", "y", "x"))
+    loads = [
+        pltpu.make_async_copy(src, dst, load_s.at[i])
+        for i, (src, dst) in enumerate((
+            (d_hbm, d_ref), (k_hbm, k_ref), (b_hbm, b_ref), (r_hbm, r_ref), (v_hbm, v_ref),
+            (gate_hbm, gate_ref), (res_hbm, res_ref), (w_hbm, w_ref),
+            (wg_hbm, wg_ref), (wu_hbm, wu_ref), (wd_hbm, wd_ref),
+        ))
+    ]
+    for copy in loads:
+        copy.start()
+    barrier = pltpu.get_barrier_semaphore()
+    plane = [(a, b) for a in range(ny) for b in range(nx) if (a, b) != (0, 0)]
+    who = [dict(c=1 - c)]
+    who += [dict(z=lax.rem(z + o, nz), c=1 - c if f else c) for o in ring_order(nz) for f in (0, 1)]
+    who += [dict(y=lax.rem(y + a, ny), x=lax.rem(x + b, nx)) for a, b in plane]
+    for where in who:
+        pl.semaphore_signal(barrier, inc=1, device_id=where, device_id_type=MESH)
+    for copy in loads[:5]:
+        copy.wait()
+    with jax.named_scope("mix"):
+        mix_body(r_ref, k_ref, v_ref, d_ref, b_ref, rd_ref, th_ref, ma_ref)
+    with jax.named_scope("meet"):
+        pl.semaphore_wait(barrier, len(who))
+        for copy in loads[5:]:
+            copy.wait()
+    flow_body(nz, ny, nx, rd_ref, th_ref, ma_ref, gate_ref, gain_ref, res_ref, ngain_ref, w_ref,
+              mid_ref, norm_ref, *rest[:FLOW_SCRATCH])
+    experts_body(nz, ny, nx, norm_ref, mid_ref, ids_ref, rw_ref, wg_ref, wu_ref, wd_ref, out_ref,
+                 *rest[FLOW_SCRATCH:])
+
+
+FLOW_SCRATCH = 21
+
+
+def layer(sizes, r, k, v, d, b, gate, gain, res, w, ngain, ids, weights, wg, wu, wd):
     nz, ny, nx = sizes
-    tokens, wide = normed.shape
+    tokens, wide = r.shape
+    part = wide // 2
+    tp = ny * nx
+    nstep = max(nz.bit_length() - 2, 0)
     ff = wg.shape[1]
     count = 2 * nz
     cap = 2 * tokens * ids.shape[1] // count
-    tp = ny * nx
     rows = 2 * cap
     dma = pltpu.SemaphoreType.DMA
     vm = pl.BlockSpec(memory_space=pltpu.VMEM)
+    hbm = pl.BlockSpec(memory_space=pl.ANY)
+    square = (tokens, wide)
+    flow_scratch = [
+        pltpu.VMEM((2 * CHUNK, part), BF16),
+        pltpu.VMEM((2 * CHUNK, part), BF16),
+        pltpu.VMEM((nstep + 1, 2 * CHUNK, part), BF16),
+        pltpu.VMEM((max(nstep, 1), 2 * CHUNK, part), BF16),
+        pltpu.VMEM((2 * CHUNK, part), BF16),
+        pltpu.VMEM((CHUNK, part), BF16),
+        pltpu.VMEM((CHUNK, part), BF16),
+        pltpu.VMEM((CHUNK, part), BF16),
+        pltpu.VMEM((CHUNK, part), BF16),
+        pltpu.VMEM((tp,) + square, BF16),
+        pltpu.VMEM(square, F32),
+        pltpu.VMEM((8, tokens), F32),
+        pltpu.VMEM((tp - 1, 8, tokens), F32),
+        dma((2,)),
+        dma((2, max(nstep, 1))),
+        dma((4,)),
+        dma((2,)),
+        dma((2 * (tp - 1),)),
+        dma((2, tp)),
+        dma((tp - 1,)),
+        dma((tp - 1,)),
+    ]
+    expert_scratch = [
+        pltpu.VMEM((count, cap, wide), BF16),
+        pltpu.VMEM((count, cap, wide), BF16),
+        pltpu.VMEM((nz, 2, rows, ff), BF16),
+        pltpu.VMEM((nx, ny, rows, ff), BF16),
+        pltpu.VMEM((ny, nx, rows, ff), BF16),
+        pltpu.VMEM((ny - 1, rows, ff), BF16),
+        pltpu.VMEM((nx - 1, rows, ff), BF16),
+        pltpu.VMEM((ny - 1, rows, ff), BF16),
+        pltpu.VMEM((nx - 1, rows, ff), BF16),
+        pltpu.VMEM((tp, rows, ff), BF16),
+        pltpu.VMEM((nz, 2, cap, wide), BF16),
+        pltpu.VMEM((count, cap, wide), BF16),
+        pltpu.VMEM((tokens, count * cap), BF16),
+        pltpu.VMEM((tokens, count * cap), BF16),
+        dma((count - 1,)),
+        dma((count,)),
+        dma((nz,)),
+        dma((nx, ny)),
+        dma((nz,)),
+        dma((ny, nx)),
+        dma((ny - 1,)),
+        dma((ny - 1,)),
+        dma((nx - 1,)),
+        dma((nx - 1,)),
+        dma((2 * (tp - 1),)),
+        dma((2, tp)),
+        dma((nz, 2)),
+        dma((count,)),
+    ]
     return pl.pallas_call(
-        functools.partial(experts_body, nz, ny, nx),
-        out_shape=jax.ShapeDtypeStruct((tokens, wide), BF16),
-        in_specs=[vm] * 7,
+        functools.partial(layer_body, nz, ny, nx),
+        out_shape=jax.ShapeDtypeStruct(square, BF16),
+        in_specs=[hbm] * 6 + [vm] + [hbm] * 2 + [vm] * 3 + [hbm] * 3,
         out_specs=vm,
-        scratch_shapes=[
-            pltpu.VMEM((count, cap, wide), BF16),
-            pltpu.VMEM((count, cap, wide), BF16),
-            pltpu.VMEM((nz, 2, rows, ff), BF16),
-            pltpu.VMEM((nx, ny, rows, ff), BF16),
-            pltpu.VMEM((ny, nx, rows, ff), BF16),
-            pltpu.VMEM((ny - 1, rows, ff), BF16),
-            pltpu.VMEM((nx - 1, rows, ff), BF16),
-            pltpu.VMEM((ny - 1, rows, ff), BF16),
-            pltpu.VMEM((nx - 1, rows, ff), BF16),
-            pltpu.VMEM((tp, rows, ff), BF16),
-            pltpu.VMEM((nz, 2, cap, wide), BF16),
-            pltpu.VMEM((count, cap, wide), BF16),
-            pltpu.VMEM((tokens, count * cap), BF16),
-            pltpu.VMEM((tokens, count * cap), BF16),
-            dma((count - 1,)),
-            dma((count,)),
-            dma((nz,)),
-            dma((nx, ny)),
-            dma((nz,)),
-            dma((ny, nx)),
-            dma((ny - 1,)),
-            dma((ny - 1,)),
-            dma((nx - 1,)),
-            dma((nx - 1,)),
-            dma((2 * (tp - 1),)),
-            dma((2, tp)),
-            dma((nz, 2)),
-            dma((count,)),
-        ],
+        scratch_shapes=[pltpu.VMEM(square, BF16)] * 7
+        + [
+            pltpu.VMEM(w.shape, BF16),
+            pltpu.VMEM(wg.shape, BF16),
+            pltpu.VMEM(wu.shape, BF16),
+            pltpu.VMEM(wd.shape, BF16),
+            pltpu.VMEM(square, F32),
+            pltpu.VMEM(square, F32),
+            pltpu.VMEM((2 * CHUNK, wide), F32),
+            pltpu.VMEM(square, BF16),
+            pltpu.VMEM(square, BF16),
+            dma((11,)),
+        ]
+        + flow_scratch
+        + expert_scratch,
         compiler_params=pltpu.CompilerParams(
-            collective_id=1, has_side_effects=True, vmem_limit_bytes=48 * 1024 * 1024
+            collective_id=0, has_side_effects=True, vmem_limit_bytes=60 * 1024 * 1024
         ),
-        name="experts",
-    )(normed, midway, ids, weights, wg, wu, wd)
+        name="layer",
+    )(r, k, v, d, b, gate, gain, res, w, ngain, ids, weights, wg, wu, wd)
 
 
 def local(
@@ -684,19 +690,25 @@
     expert_up,
     expert_down,
 ):
-    reads, through, ends = mix_local(
-        receptance, key_vectors, value_vectors, decay_logits, rate_logits
-    )
-    tokens_here, features = residual.shape
     sizes = tuple(lax.axis_size(name) for name in ("z", "y", "x"))
-    planes = sizes[1] * sizes[2]
-    midway, normed = flow(
-        sizes, reads, through, ends, gate_logits, group_gain[None], residual, norm_gain[None],
-        mixer_out.reshape(planes, -1, features),
-    )
-    return experts(
-        sizes, normed, midway, expert_ids, route_weight,
-        expert_gate[0], expert_up[0], expert_down[0],
+    features = residual.shape[1]
+    return layer(
+        sizes,
+        receptance,
+        key_vectors,
+        value_vectors,
+        decay_logits,
+        rate_logits,
+        gate_logits,
+        group_gain[None],
+        residual,
+        mixer_out.reshape(sizes[1] * sizes[2], -1, features),
+        norm_gain[None],
+        expert_ids,
+        route_weight,
+        expert_gate[0],
+        expert_up[0],
+        expert_down[0],
     )
 
 

time: 175 us -> 161 us (0.920)
  Pallas kernels: 164 us -> 156 us
  local copies, waits for them, and re-layouts: 10.3 us -> 4.5 us
    pallas_call x3 -> x1, Pallas kernels: 164 us -> 156 us  [layer(): pl.pallas_call(functools.partial(layer_body, nz, ny, nx), out_shape=jax.S...]
    unnamed x33 -> x3, local copies, waits for them, and re-layouts: 10.3 us -> 4.5 us
where the time goes in v4:
time: 161 us; the launch traced here: 160 us
  Pallas kernels  156 us (97%)
  local copies, waits for them, and re-layouts  4.5 us (3%)
    pallas_call x1, Pallas kernels, layer(): pl.pallas_call(functools.partial(layer_body, nz, ny, nx), out_shape=jax.S...  156 us
    unnamed x3, local copies, waits for them, and re-layouts  4.5 us

profile of v4, /device:TPU:21, one launch (start us, length us, event | category | flops | bytes accessed | tf_op | source)
XLA Modules:
  0.0 160.5 jit_solution(11730266172351866588)
XLA Ops:
  0.0 1.5 copy.16.ids_ref
  1.5 1.5 copy.17.rw_ref
  2.9 156.0 %layer.1 = bf16[256,256]{1,0:T(8,128)(2,1)} custom-call(bf16[256,256]{1,0:T(8,128)(2,1)} %r_hbm.1, bf16[256,256]{1,0:T(8,128)(2,1)} %k_hbm.1, bf16[256,256]{1,0:T(8,128)(2,1)} %v_hbm.1, bf16[256,256]{1,0:T(8,128)(2,1)} %d_hbm.1, bf16[256,256]{1,0:T(8,128)(2,1)} %b_hbm.1, bf16[256,256]{1,0:T(8,128)(2,1)} %gate_hbm.1, f32[1,256]{1,0:T(1,128)} %bitcast.10, ...), custom_call_target="tpu_custom_call" | custom-call | tf_op jit(solution)/shard_map/layer/pallas_call | solution.py:649
  158.9 1.6 copy.19

commit v5 on v4

--- a/solution.py
+++ b/solution.py
@@ -195,45 +195,36 @@
         push(mine, 0, y=lax.rem(y + k, ny))
     for k in xs:
         push(mine, 1, x=lax.rem(x + k, nx))
-    use(mine, 0)
-    use(mine, 1)
+    use(mine, 0, 0, 0)
+    use(mine, 1, 0, 0)
     for k in range(max(len(xs), len(ys))):
         if k < len(xs):
             slot = y * nx + lax.rem(x + nx - xs[k], nx)
             arrived(slot, 0)
             for j in ys:
                 push(slot, 0, y=lax.rem(y + j, ny))
-            use(slot, 0)
+            use(slot, 0, 0, xs[k])
         if k < len(ys):
             slot = lax.rem(y + ny - ys[k], ny) * nx + x
             arrived(slot, 1)
             for j in xs:
                 push(slot, 1, x=lax.rem(x + j, nx))
-            use(slot, 1)
-    for k in ys:
-        slot = lax.rem(y + ny - k, ny) * nx + x
-        arrived(slot, 0)
-        use(slot, 0)
-    for k in xs:
-        slot = y * nx + lax.rem(x + nx - k, nx)
-        arrived(slot, 1)
-        use(slot, 1)
-    for a in xs:
-        for b in ys:
-            for part, (j, k) in ((0, (b, a)), (1, (b, a))):
-                slot = lax.rem(y + ny - j, ny) * nx + lax.rem(x + nx - k, nx)
-                arrived(slot, part)
-                use(slot, part)
+            use(slot, 1, ys[k], 0)
+    for a in range(max(len(xs), len(ys))):
+        for b in range(max(nx, ny)):
+            if a < len(ys) and b < nx:
+                slot = lax.rem(y + ny - ys[a], ny) * nx + lax.rem(x + nx - b, nx)
+                arrived(slot, 0)
+                use(slot, 0, ys[a], b)
+            if a < len(xs) and b < ny:
+                slot = lax.rem(y + ny - b, ny) * nx + lax.rem(x + nx - xs[a], nx)
+                arrived(slot, 1)
+                use(slot, 1, b, xs[a])
     return sent
 
 
-def exact_left(a, b, mask, dims=NN):
-    b_hi, b_lo = halves(b)
-    return dot_dims(a, block_diag(b_hi, mask), dims) + dot_dims(a, block_diag(b_lo, mask), dims)
-
-
 def flow_body(nz, ny, nx, rd_ref, th_ref, ma_ref, gate_ref, gain_ref, res_ref, ngain_ref, w_ref,
-              mid_ref, norm_ref,
+              mid_ref, norm_ref, meanwhile,
               pair_out, pair_in, hop_out, hop_in, near_in, far_out, far_in, back_out, back_in,
               blocks, total, sq_out, sq_in,
               pair_s, hop_s, fin_s, back_s, ag_send, ag_recv, sq_send, sq_recv):
@@ -271,6 +262,8 @@
         hop_out[i] = cur.astype(BF16)
         hop = remote(hop_out.at[i], hop_in.at[i], hop_s.at[0, i], hop_s.at[1, i], z=lax.rem(z + d, nz))
         hop.start()
+        if d == steps[-1]:
+            meanwhile()
         with jax.named_scope(f"hop{d}"):
             hop.wait()
         joined = compose(hop_in[i].astype(F32), cur)
@@ -310,7 +303,7 @@
     total[...] = res_ref[...].astype(F32)
     half = blocks.shape[1] // 2
 
-    def project(slot, part_no):
+    def project(slot, part_no, *place):
         rows = pl.ds(part_no * half, half)
         total[rows, :] += jnp.dot(blocks[slot, rows, :], w_ref[slot], preferred_element_type=F32)
 
@@ -329,38 +322,53 @@
                       y=lax.rem(y + a, ny), x=lax.rem(x + b, nx))
         copy.start()
         pieces.append(copy)
-    with jax.named_scope("squares"):
+    norm_ref[...] = (mid_f * ngain_ref[...]).astype(BF16)
+
+    def inverse_rms():
+        total_sq = sq_out[...]
         for i, copy in enumerate(pieces):
             copy.wait_recv()
-            sums = sums + sq_in[i]
-    t_hi, t_lo = halves(sums)
-    t_mid, t_lo = halves(sums - t_hi.astype(F32))
-    eighth = jnp.full((8, wide), 0.125, BF16)
-    squares = dot_dims(t_hi, eighth, TN) + dot_dims(t_mid, eighth, TN) + dot_dims(t_lo, eighth, TN)
-    inv = lax.rsqrt(squares * (1.0 / (wide * ny * nx)) + EPS_NORM)
-    norm_ref[...] = (mid_f * ngain_ref[...] * inv).astype(BF16)
-    for copy in sent + pieces:
-        copy.wait_send()
-
-
-def experts_body(nz, ny, nx, norm_ref, mid_ref, ids_ref, rw_ref, wg_ref, wu_ref, wd_ref, out_ref,
-                 going, came, parts, from_x, from_y, sum_a, sum_b, last_a, last_b, hid, res, back,
-                 pick_hi, pick_lo,
-                 go_s, go_r, x_s, x_r, y_s, y_r, a_s, a_r, b_s, b_r, ag_send, ag_recv, re_s, re_r):
-    z, c, y, x = (lax.axis_index(name) for name in ("z", "c", "y", "x"))
-    me = 2 * z + c
-    tp = y * nx + x
-    tokens = norm_ref.shape[0]
-    count, cap, _ = going.shape
-    slots = count * cap
+            total_sq = total_sq + sq_in[i]
+        return lax.rsqrt(total_sq * (1.0 / (wide * ny * nx)) + EPS_NORM)
+
+    return inverse_rms, sent + pieces
+
+
+def trade_weights(ny, nx, wg_ref, wu_ref, w_a, w_b, wt_s, wt_r):
+    y, x = lax.axis_index("y"), lax.axis_index("x")
     ff = wg_ref.shape[1]
-    hf = ff // 2
-    xs, ys = ring_order(nx), ring_order(ny)
-    zs = ring_order(nz)
-
-    def core_of(flip):
-        return 1 - c if flip else c
-
+    copies = []
+    for part, (name, at, n, dst) in enumerate((("x", x, nx, w_a), ("y", y, ny, w_b))):
+        cut = ff // n
+        for k in ring_order(n):
+            to = lax.rem(at + k, n)
+            cols = pl.ds(pl.multiple_of(to * cut, cut), cut)
+            for which, src in enumerate((wg_ref, wu_ref)):
+                copy = remote(src.at[:, cols], dst.at[at, which], wt_s.at[part, which, to],
+                              wt_r.at[part, which, at], **{name: to})
+                copy.start()
+                copies.append(copy)
+    for part, (at, n, dst) in enumerate(((x, nx, w_a), (y, ny, w_b))):
+        cut = ff // n
+        cols = pl.ds(pl.multiple_of(at * cut, cut), cut)
+        dst[at, 0] = wg_ref[:, cols]
+        dst[at, 1] = wu_ref[:, cols]
+
+    def finish():
+        for copy in copies:
+            copy.wait_send()
+        for part, (at, n, dst) in enumerate(((x, nx, w_a), (y, ny, w_b))):
+            for k in ring_order(n):
+                src = lax.rem(at + k, n)
+                for which in (0, 1):
+                    got = dst.at[src, which]
+                    remote(got, got, wt_s.at[part, which, 0], wt_r.at[part, which, src], c=1 - lax.axis_index("c")).wait_recv()
+
+    return finish
+
+
+def prepare_routes(cap, slots, ids_ref, rw_ref, taken, turned, pick_hi, pick_lo):
+    tokens = ids_ref.shape[0]
     ids = ids_ref[...]
     id0, id1 = ids[:, 0:1], ids[:, 1:2]
     lane = iota2((tokens, 128), 1)
@@ -372,135 +380,218 @@
         rank = jnp.sum(jnp.where(lane == one, earlier, 0.0), axis=1, keepdims=True)
         return one * cap + rank.astype(jnp.int32)
 
-    with jax.named_scope("route"):
-        slot0, slot1 = slot_of(id0), slot_of(id1)
+    slot0, slot1 = slot_of(id0), slot_of(id1)
     spot = iota2((tokens, slots), 1)
     hot0, hot1 = spot == slot0, spot == slot1
     take = jnp.where(hot0 | hot1, 1.0, 0.0).astype(BF16)
-    going[...] = dot_dims(take, norm_ref[...], TN).astype(BF16).reshape(going.shape)
-
-    sent = []
-
-    def dispatch(zt, ct):
-        e = 2 * zt + ct
-        copy = remote(going.at[e], came.at[me], go_s.at[len(sent)], go_r.at[me], z=zt, c=ct)
-        copy.start()
-        sent.append(copy)
-
-    came[me] = going[me]
-    dispatch(z, 1 - c)
-    for o in zs:
-        for f in (0, 1):
-            dispatch(lax.rem(z + o, nz), core_of(f))
     rw = rw_ref[...]
     weight = jnp.where(hot0, rw[:, 0:1], 0.0) + jnp.where(hot1, rw[:, 1:2], 0.0)
     w_hi, w_lo = halves(weight)
     pick_hi[...] = w_hi
     pick_lo[...] = w_lo
+    taken[...] = take
+    eye = (iota2((tokens, tokens), 0) == iota2((tokens, tokens), 1)).astype(F32).astype(BF16)
+    turned[...] = dot_dims(take, eye, TN).astype(BF16)
+
+
+def experts_body(nz, ny, nx, inverse_rms, norm_ref, mid_ref, w_a, w_b, wd_ref, out_ref,
+                 taken, turned, pick_hi, pick_lo, going, came, rows_a, rows_b, half_a, half_b, got_a, got_b, own_a, own_b,
+                 hid, res, back, scale_out, scale_in, scale_col,
+                 go_s, go_r, x_s, x_r, y_s, y_r, a_s, a_r, b_s, b_r, ag_send, ag_recv, re_s, re_r, sc_s, sc_r):
+    z, c, y, x = (lax.axis_index(name) for name in ("z", "c", "y", "x"))
+    me = 2 * z + c
+    tp = y * nx + x
+    count, cap, wide = going.shape
+    slots = count * cap
+    xs, ys = ring_order(nx), ring_order(ny)
+
+    going[...] = dot_dims(turned[...], norm_ref[...], NN).astype(BF16).reshape(going.shape)
+
+    nh = nz // 2
+    offs = [0] + [o for d in range(1, nh) for o in (d, nz - d)] + [nh]
+    sent = []
+
+    def dispatch(zt, ct):
+        copy = remote(going.at[2 * zt + ct], came.at[me], go_s.at[len(sent)], go_r.at[me], z=zt, c=ct)
+        copy.start()
+        sent.append(copy)
+
+    def dispatch_to(ct):
+        for o in offs[1:]:
+            dispatch(lax.rem(z + nz - o, nz), ct)
+
+    came[me] = going[me]
+    dispatch(z, 1 - c)
+    dispatch_to(0)
+    group = 128 // cap
+    line = jnp.where(c == 0, lax.div(z, nx), lax.rem(z, nx))
+    speaks = line == jnp.where(c == 0, y, x)
+    place = jnp.where(c == 0, lax.rem(z, nx), lax.div(z, nx))
+
+    def scale_to(e):
+        return remote(scale_out.at[lax.div(e, group)], scale_in.at[c, place], sc_s.at[e], sc_r.at[c, place],
+                      z=lax.div(e, 2), c=lax.rem(e, 2))
+
+    def tell_scale():
+        inv = inverse_rms()
+        i_hi, i_rest = halves(inv)
+        i_mid, i_lo = halves(inv - i_hi.astype(F32))
+        spread = (dot_dims(i_hi, taken[...], NN) + dot_dims(i_mid, taken[...], NN)
+                  + dot_dims(i_lo, taken[...], NN))
+        for g in range(slots // 128):
+            scale_out[g] = spread[:, g * 128 : (g + 1) * 128]
+
+        @pl.when(speaks)
+        def _():
+            def tell(e, carry):
+                @pl.when(e != me)
+                def _():
+                    scale_to(e).start()
+
+                return carry
+
+            lax.fori_loop(0, count, tell, 0)
+            scale_in[c, place] = scale_out[lax.div(me, group)]
+
+    tell_scale()
+    dispatch_to(1)
 
     def take_in(src):
         @pl.when(src != me)
         def _():
             remote(came.at[src], came.at[src], go_s.at[0], go_r.at[src], c=1 - c).wait_recv()
 
-    def to_x(t):
-        xt, yt = lax.rem(t, nx), lax.div(t, nx)
-        return remote(parts.at[t, 0], from_x.at[x, yt], x_s.at[t], x_r.at[x, yt], x=xt)
-
-    def to_y(t):
-        xt, yt = lax.rem(t, nx), lax.div(t, nx)
-        return remote(parts.at[t, 1], from_y.at[y, xt], y_s.at[t], y_r.at[y, xt], y=yt)
-
-    def gate_up(k, carry):
-        off = jnp.where(lax.rem(k, 2) == 1, lax.div(k + 1, 2), nz - lax.div(k, 2))
-        t = lax.rem(z + off, nz)
+    def onward(t):
+        copies = [remote(came.at[2 * t], rows_a.at[x, t], x_s.at[k - 1, t], x_r.at[x, t], x=lax.rem(x + k, nx))
+                  for k in xs]
+        copies += [remote(came.at[2 * t + 1], rows_b.at[y, t], y_s.at[k - 1, t], y_r.at[y, t], y=lax.rem(y + k, ny))
+                   for k in ys]
+        return copies
+
+    def receive(t):
         take_in(2 * t)
         take_in(2 * t + 1)
-        rows = came[pl.ds(2 * t, 2)].reshape(2 * cap, came.shape[2])
-        gate = jnp.dot(rows, wg_ref[...], preferred_element_type=F32).astype(BF16)
-        up = jnp.dot(rows, wu_ref[...], preferred_element_type=F32).astype(BF16)
-        parts[t, 0, :, :hf] = gate[:, :hf]
-        parts[t, 0, :, hf:] = up[:, :hf]
-        parts[t, 1, :, :hf] = gate[:, hf:]
-        parts[t, 1, :, hf:] = up[:, hf:]
-
-        @pl.when(lax.rem(t, nx) != x)
+        for copy in onward(t):
+            copy.start()
+
+    def settle_a(t):
+        ty, tx = lax.div(t, nx), lax.rem(t, nx)
+        return remote(half_a.at[t], got_a.at[y, tx], a_s.at[t], a_r.at[y, tx], y=ty)
+
+    def settle_b(t):
+        ty, tx = lax.div(t, nx), lax.rem(t, nx)
+        return remote(half_b.at[t], got_b.at[x, ty], b_s.at[t], b_r.at[x, ty], x=tx)
+
+    def partials(t):
+        ty, tx = lax.div(t, nx), lax.rem(t, nx)
+        for part, (places, at, n, rows, recv, w, out, own, mine, spot_own, settle) in enumerate((
+            (xs, x, nx, rows_a, x_r, w_a, half_a, own_a, ty == y, tx, settle_a),
+            (ys, y, ny, rows_b, y_r, w_b, half_b, own_b, tx == x, ty, settle_b),
+        )):
+            first = came[2 * t + part]
+            gate = jnp.dot(first, w[at, 0], preferred_element_type=F32)
+            up = jnp.dot(first, w[at, 1], preferred_element_type=F32)
+            for k in places:
+                src = lax.rem(at + n - k, n)
+                got = rows.at[src, t]
+                remote(got, got, go_s.at[0], recv.at[src, t], c=1 - c).wait_recv()
+                value = rows[src, t]
+                gate = gate + jnp.dot(value, w[src, 0], preferred_element_type=F32)
+                up = up + jnp.dot(value, w[src, 1], preferred_element_type=F32)
+            cut = gate.shape[1]
+
+            @pl.when(mine)
+            def _(own=own, spot_own=spot_own, gate=gate, up=up, cut=cut):
+                own[spot_own, :, :cut] = gate
+                own[spot_own, :, cut:] = up
+
+            @pl.when(jnp.logical_not(mine))
+            def _(out=out, settle=settle, gate=gate, up=up, cut=cut):
+                out[t, :, :cut] = gate.astype(BF16)
+                out[t, :, cut:] = up.astype(BF16)
+                settle(t).start()
+
+    def block_at(i):
+        d = lax.div(i + 1, 2)
+        off = jnp.where(lax.rem(i, 2) == 1, d, lax.rem(nz - d, nz))
+        return lax.rem(z + off, nz)
+
+    def step(j, carry):
+        @pl.when(j < nz)
         def _():
-            to_x(t).start()
-
-        @pl.when(lax.div(t, nx) != y)
+            receive(block_at(j))
+
+        @pl.when(j >= LAG)
         def _():
-            to_y(t).start()
+            partials(block_at(j - LAG))
 
         return carry
 
-    with jax.named_scope("gateup"):
-        lax.fori_loop(0, nz, gate_up, 0)
-
-    def added_a(yb):
-        acc = parts[yb * nx + x, 0].astype(F32)
-        for k in xs:
-            src = lax.rem(x + nx - k, nx)
-            remote(from_x.at[src, yb], from_x.at[src, yb], x_s.at[0], x_r.at[src, yb], x=src).wait_recv()
-            acc = acc + from_x[src, yb].astype(F32)
-        return acc
-
-    def added_b(xb):
-        acc = parts[y * nx + xb, 1].astype(F32)
-        for k in ys:
-            src = lax.rem(y + ny - k, ny)
-            remote(from_y.at[src, xb], from_y.at[src, xb], y_s.at[0], y_r.at[src, xb], y=src).wait_recv()
-            acc = acc + from_y[src, xb].astype(F32)
-        return acc
-
-    second = []
-    with jax.named_scope("second"):
-        for k in range(max(len(xs), len(ys))):
-            if k < len(ys):
-                yb = lax.rem(y + ys[k], ny)
-                sum_a[k] = added_a(yb).astype(BF16)
-                copy = remote(sum_a.at[k], last_a.at[k], a_s.at[k], a_r.at[k], y=yb)
-                copy.start()
-                second.append(copy)
-            if k < len(xs):
-                xb = lax.rem(x + xs[k], nx)
-                sum_b[k] = added_b(xb).astype(BF16)
-                copy = remote(sum_b.at[k], last_b.at[k], b_s.at[k], b_r.at[k], x=xb)
-                copy.start()
-                second.append(copy)
-    tot_a = added_a(y)
-    tot_b = added_b(x)
-    with jax.named_scope("last"):
-        for copy in second:
-            copy.wait_recv()
-    for k in range(len(ys)):
-        tot_a = tot_a + last_a[k].astype(F32)
-    for k in range(len(xs)):
-        tot_b = tot_b + last_b[k].astype(F32)
-
-    def act(both):
-        gate, up = both[:, :hf], both[:, hf:]
-        return (gate / (1.0 + jnp.exp(-gate)) * up).astype(BF16)
-
-    hid[tp, :, :hf] = act(tot_a)
-    hid[tp, :, hf:] = act(tot_b)
-
-    def give_back(slot, part):
-        return remote(res.at[slot, part], back.at[me], re_s.at[slot, part], re_r.at[me], z=slot, c=part)
-
-    def down(slot, part):
-        rows = hid[slot, pl.ds(part * cap, cap), :]
-        value = jnp.dot(rows, wd_ref[...], preferred_element_type=F32).astype(BF16)
-        res[slot, part] = value
-        own = jnp.logical_and(slot == z, c == part)
-
-        @pl.when(own)
-        def _():
-            back[me] = value
-
-        @pl.when(jnp.logical_not(own))
-        def _():
-            give_back(slot, part).start()
+    with jax.named_scope("pipeline"):
+        lax.fori_loop(0, nz + LAG, step, 0)
+
+    eighth = jnp.full((8, 128), 0.125, BF16)
+    with jax.named_scope("activate"):
+        for part, (places, at, n, m, got, recv, own) in enumerate((
+            (ys, y, ny, nx, got_a, a_r, own_a),
+            (xs, x, nx, ny, got_b, b_r, own_b),
+        )):
+            for i in range(m):
+                from_z = y * nx + i if part == 0 else i * nx + x
+
+                @pl.when(jnp.logical_not(jnp.logical_and(from_z == z, c == part)))
+                def _(part=part, i=i):
+                    ref = scale_in.at[part, i]
+                    remote(ref, ref, sc_s.at[0], sc_r.at[part, i], c=1 - c).wait_recv()
+
+                s_hi, s_rest = halves(scale_in[part, i])
+                s_mid, s_lo = halves(scale_in[part, i] - s_hi.astype(F32))
+                scale_col[...] = dot_dims(s_hi, eighth, TN) + dot_dims(s_mid, eighth, TN) + dot_dims(s_lo, eighth, TN)
+                factor = scale_col[pl.ds(pl.multiple_of(lax.rem(me, group) * cap, cap), cap), :]
+                total = own[i]
+                cut = total.shape[1] // 2
+                for k in places:
+                    src = lax.rem(at + n - k, n)
+                    ref = got.at[src, i]
+                    remote(ref, ref, go_s.at[0], recv.at[src, i], c=1 - c).wait_recv()
+                    total = total + got[src, i].astype(F32)
+                total = total * jnp.concatenate([factor] * (2 * cut // 128), axis=1)
+                gate, up = total[:, :cut], total[:, cut:]
+                first_row = part * m * cap + i * cap
+                hid[tp, first_row : first_row + cap, :] = (gate / (1.0 + jnp.exp(-gate)) * up).astype(BF16)
+
+    def give_back(t, part):
+        return remote(res.at[t, part], back.at[me], re_s.at[t, part], re_r.at[me], z=t, c=part)
+
+    seen = {}
+    half_rows = hid.shape[1] // 2
+
+    def down(slot, part, dy, dx):
+        key = (part, dy if part == 0 else dx)
+        seen[key] = seen.get(key, 0) + 1
+        n = nx if part == 0 else ny
+        if seen[key] < n:
+            return
+        ry, rx = lax.rem(y + ny - dy, ny), lax.rem(x + nx - dx, nx)
+        value = None
+        for k in range(n):
+            src = ry * nx + k if part == 0 else k * nx + rx
+            term = jnp.dot(hid[src, part * half_rows : (part + 1) * half_rows, :], wd_ref[k], preferred_element_type=F32)
+            value = term if value is None else value + term
+        value = value.astype(BF16)
+        for i in range(n):
+            t = ry * nx + i if part == 0 else i * nx + rx
+            piece = value[i * cap : (i + 1) * cap]
+            res[t, part] = piece
+            here = jnp.logical_and(t == z, c == part)
+
+            @pl.when(here)
+            def _(piece=piece):
+                back[me] = piece
+
+            @pl.when(jnp.logical_not(here))
+            def _(t=t):
+                give_back(t, part).start()
 
     with jax.named_scope("down"):
         shared = share_blocks(hid, ag_send, ag_recv, y, x, ny, nx, down)
@@ -514,31 +605,44 @@
 
     with jax.named_scope("collect"):
         lax.fori_loop(0, count, collect, 0)
-    rows = back[...].reshape(slots, back.shape[2])
+    rows = back[...].reshape(slots, wide)
     routed = dot_dims(pick_hi[...], rows, NN) + dot_dims(pick_lo[...], rows, NN)
     out_ref[...] = (mid_ref[...].astype(F32) + routed).astype(BF16)
 
-    for copy in sent + second + shared:
+    for copy in sent + shared:
         copy.wait_send()
 
     def drain(t, carry):
+        for copy in onward(t):
+            copy.wait_send()
+
+        @pl.when(lax.div(t, nx) != y)
+        def _():
+            settle_a(t).wait_send()
+
         @pl.when(lax.rem(t, nx) != x)
         def _():
-            to_x(t).wait_send()
-
-        @pl.when(lax.div(t, nx) != y)
-        def _():
-            to_y(t).wait_send()
+            settle_b(t).wait_send()
 
         for part in (0, 1):
             @pl.when(jnp.logical_not(jnp.logical_and(t == z, c == part)))
-            def _():
+            def _(part=part):
                 give_back(t, part).wait_send()
+
+            e = 2 * t + part
+
+            @pl.when(jnp.logical_and(speaks, e != me))
+            def _(e=e):
+                scale_to(e).wait_send()
 
         return carry
 
     with jax.named_scope("drain"):
         lax.fori_loop(0, nz, drain, 0)
+
+
+LAG = 6
+
 
 def layer_body(nz, ny, nx, r_hbm, k_hbm, v_hbm, d_hbm, b_hbm, gate_hbm, gain_ref, res_hbm, w_hbm, ngain_ref,
                ids_ref, rw_ref, wg_hbm, wu_hbm, wd_hbm, out_ref,
@@ -570,10 +674,18 @@
         pl.semaphore_wait(barrier, len(who))
         for copy in loads[5:]:
             copy.wait()
-    flow_body(nz, ny, nx, rd_ref, th_ref, ma_ref, gate_ref, gain_ref, res_ref, ngain_ref, w_ref,
-              mid_ref, norm_ref, *rest[:FLOW_SCRATCH])
-    experts_body(nz, ny, nx, norm_ref, mid_ref, ids_ref, rw_ref, wg_ref, wu_ref, wd_ref, out_ref,
-                 *rest[FLOW_SCRATCH:])
+    routes = rest[FLOW_SCRATCH + 4 : FLOW_SCRATCH + 8]
+    slots, cap = routes[1].shape[0], routes[1].shape[0] // (2 * nz)
+    meanwhile = functools.partial(prepare_routes, cap, slots, ids_ref, rw_ref, *routes)
+    finish_trade = trade_weights(ny, nx, wg_ref, wu_ref, *rest[FLOW_SCRATCH : FLOW_SCRATCH + 4])
+    inverse_rms, sent = flow_body(nz, ny, nx, rd_ref, th_ref, ma_ref, gate_ref, gain_ref, res_ref, ngain_ref, w_ref,
+              mid_ref, norm_ref, meanwhile, *rest[:FLOW_SCRATCH])
+    finish_trade()
+    w_a, w_b = rest[FLOW_SCRATCH], rest[FLOW_SCRATCH + 1]
+    experts_body(nz, ny, nx, inverse_rms, norm_ref, mid_ref, w_a, w_b, wd_ref, out_ref,
+                 *rest[FLOW_SCRATCH + 4 :])
+    for copy in sent:
+        copy.wait_send()
 
 
 FLOW_SCRATCH = 21
@@ -589,6 +701,7 @@
     count = 2 * nz
     cap = 2 * tokens * ids.shape[1] // count
     rows = 2 * cap
+    wd = wd.reshape(nx, ff // nx, wide)
     dma = pltpu.SemaphoreType.DMA
     vm = pl.BlockSpec(memory_space=pltpu.VMEM)
     hbm = pl.BlockSpec(memory_space=pl.ANY)
@@ -616,35 +729,50 @@
         dma((tp - 1,)),
         dma((tp - 1,)),
     ]
+    cut = ff // nx
+    trade_scratch = [
+        pltpu.VMEM((nx, 2, wide, cut), BF16),
+        pltpu.VMEM((ny, 2, wide, cut), BF16),
+        dma((2, 2, nx)),
+        dma((2, 2, nx)),
+    ]
     expert_scratch = [
+        pltpu.VMEM((tokens, count * cap), BF16),
+        pltpu.VMEM((count * cap, tokens), BF16),
+        pltpu.VMEM((tokens, count * cap), BF16),
+        pltpu.VMEM((tokens, count * cap), BF16),
         pltpu.VMEM((count, cap, wide), BF16),
         pltpu.VMEM((count, cap, wide), BF16),
-        pltpu.VMEM((nz, 2, rows, ff), BF16),
-        pltpu.VMEM((nx, ny, rows, ff), BF16),
-        pltpu.VMEM((ny, nx, rows, ff), BF16),
-        pltpu.VMEM((ny - 1, rows, ff), BF16),
-        pltpu.VMEM((nx - 1, rows, ff), BF16),
-        pltpu.VMEM((ny - 1, rows, ff), BF16),
-        pltpu.VMEM((nx - 1, rows, ff), BF16),
-        pltpu.VMEM((tp, rows, ff), BF16),
+        pltpu.VMEM((nx, nz, cap, wide), BF16),
+        pltpu.VMEM((ny, nz, cap, wide), BF16),
+        pltpu.VMEM((nz, cap, 2 * cut), BF16),
+        pltpu.VMEM((nz, cap, 2 * cut), BF16),
+        pltpu.VMEM((ny, nx, cap, 2 * cut), BF16),
+        pltpu.VMEM((nx, ny, cap, 2 * cut), BF16),
+        pltpu.VMEM((nx, cap, 2 * cut), F32),
+        pltpu.VMEM((ny, cap, 2 * cut), F32),
+        pltpu.VMEM((tp, 2 * nx * cap, cut), BF16),
         pltpu.VMEM((nz, 2, cap, wide), BF16),
         pltpu.VMEM((count, cap, wide), BF16),
-        pltpu.VMEM((tokens, count * cap), BF16),
-        pltpu.VMEM((tokens, count * cap), BF16),
+        pltpu.VMEM((count * cap // 128, 8, 128), F32),
+        pltpu.VMEM((2, nx, 8, 128), F32),
+        pltpu.VMEM((128, 128), F32),
         dma((count - 1,)),
         dma((count,)),
+        dma((nx - 1, nz)),
+        dma((nx, nz)),
+        dma((ny - 1, nz)),
+        dma((ny, nz)),
+        dma((nz,)),
+        dma((ny, nx)),
         dma((nz,)),
         dma((nx, ny)),
-        dma((nz,)),
-        dma((ny, nx)),
-        dma((ny - 1,)),
-        dma((ny - 1,)),
-        dma((nx - 1,)),
-        dma((nx - 1,)),
         dma((2 * (tp - 1),)),
         dma((2, tp)),
         dma((nz, 2)),
         dma((count,)),
+        dma((count,)),
+        dma((2, nx)),
     ]
     return pl.pallas_call(
         functools.partial(layer_body, nz, ny, nx),
@@ -665,6 +793,7 @@
             dma((11,)),
         ]
         + flow_scratch
+        + trade_scratch
         + expert_scratch,
         compiler_params=pltpu.CompilerParams(
             collective_id=0, has_side_effects=True, vmem_limit_bytes=60 * 1024 * 1024

time: 161 us -> 139 us (0.86)
  the two profiles are of different devices: /device:TPU:21 before, /device:TPU:33 now
where the time goes in v5:
time: 139 us
  Pallas kernels  135 us (97%)
  local copies, waits for them, and re-layouts  4.5 us (3%)
    pallas_call x1, Pallas kernels, layer(): pl.pallas_call(functools.partial(layer_body, nz, ny, nx), out_shape=jax.S...  135 us
    unnamed x3, local copies, waits for them, and re-layouts  4.5 us

profile of v5, /device:TPU:33, one launch (start us, length us, event | category | flops | bytes accessed | tf_op | source)
XLA Modules:
  0.0 139.1 jit_solution(10761753691147985310)
XLA Ops:
  0.0 1.5 %copy.16.ids_ref = s32[256,2]{1,0:T(8,128)} copy(s32[256,2]{0,1:T(2,128)} %param.25) | data formatting | bytes 4096 | tf_op args[10]
  1.5 1.5 %copy.17.rw_ref = f32[256,2]{1,0:T(8,128)} copy(f32[256,2]{0,1:T(2,128)} %param.26) | data formatting | bytes 4096 | tf_op args[11]
  2.9 134.6 %layer.1 = bf16[256,256]{1,0:T(8,128)(2,1)} custom-call(bf16[256,256]{1,0:T(8,128)(2,1)} %r_hbm.1, bf16[256,256]{1,0:T(8,128)(2,1)} %k_hbm.1, bf16[256,256]{1,0:T(8,128)(2,1)} %v_hbm.1, bf16[256,256]{1,0:T(8,128)(2,1)} %d_hbm.1, bf16[256,256]{1,0:T(8,128)(2,1)} %b_hbm.1, bf16[256,256]{1,0:T(8,128)(2,1)} %gate_hbm.1, f32[1,256]{1,0:T(1,128)} %bitcast.10, ...), custom_call_target="tpu_custom_call" | custom-call | tf_op jit(solution)/shard_map/layer/pallas_call | solution.py:777
  137.5 1.6 %copy.19 = bf16[256,256]{1,0:T(8,128)(2,1)} copy(bf16[256,256]{1,0:T(8,128)(2,1)} %layer.1) | data formatting | bytes 262144

commit v6 on v5

--- a/solution.py
+++ b/solution.py
@@ -531,23 +531,28 @@
         lax.fori_loop(0, nz + LAG, step, 0)
 
     eighth = jnp.full((8, 128), 0.125, BF16)
+    with jax.named_scope("scales"):
+        for part, m in ((0, nx), (1, ny)):
+            for i in range(m):
+                from_z = y * nx + i if part == 0 else i * nx + x
+
+                @pl.when(jnp.logical_not(jnp.logical_and(from_z == z, c == part)))
+                def _(part=part, i=i):
+                    ref = scale_in.at[part, i]
+                    remote(ref, ref, sc_s.at[0], sc_r.at[part, i], c=1 - c).wait_recv()
+
+        for part, m in ((0, nx), (1, ny)):
+            for i in range(m):
+                s_hi, s_rest = halves(scale_in[part, i])
+                s_mid, s_lo = halves(scale_in[part, i] - s_hi.astype(F32))
+                scale_col[part, i] = dot_dims(s_hi, eighth, TN) + dot_dims(s_mid, eighth, TN) + dot_dims(s_lo, eighth, TN)
     with jax.named_scope("activate"):
         for part, (places, at, n, m, got, recv, own) in enumerate((
             (ys, y, ny, nx, got_a, a_r, own_a),
             (xs, x, nx, ny, got_b, b_r, own_b),
         )):
             for i in range(m):
-                from_z = y * nx + i if part == 0 else i * nx + x
-
-                @pl.when(jnp.logical_not(jnp.logical_and(from_z == z, c == part)))
-                def _(part=part, i=i):
-                    ref = scale_in.at[part, i]
-                    remote(ref, ref, sc_s.at[0], sc_r.at[part, i], c=1 - c).wait_recv()
-
-                s_hi, s_rest = halves(scale_in[part, i])
-                s_mid, s_lo = halves(scale_in[part, i] - s_hi.astype(F32))
-                scale_col[...] = dot_dims(s_hi, eighth, TN) + dot_dims(s_mid, eighth, TN) + dot_dims(s_lo, eighth, TN)
-                factor = scale_col[pl.ds(pl.multiple_of(lax.rem(me, group) * cap, cap), cap), :]
+                factor = scale_col[part, i, pl.ds(pl.multiple_of(lax.rem(me, group) * cap, cap), cap), :]
                 total = own[i]
                 cut = total.shape[1] // 2
                 for k in places:
@@ -756,7 +761,7 @@
         pltpu.VMEM((count, cap, wide), BF16),
         pltpu.VMEM((count * cap // 128, 8, 128), F32),
         pltpu.VMEM((2, nx, 8, 128), F32),
-        pltpu.VMEM((128, 128), F32),
+        pltpu.VMEM((2, nx, 128, 128), F32),
         dma((count - 1,)),
         dma((count,)),
         dma((nx - 1, nz)),

time: 139 us -> 138 us (level)
  the two profiles are of different devices: /device:TPU:33 before, /device:TPU:1 now
where the time goes in v6:
time: 138 us; the launch traced here: 135 us
  Pallas kernels  131 us (95%)
  local copies, waits for them, and re-layouts  4.5 us (3%)
    pallas_call x1, Pallas kernels, layer(): pl.pallas_call(functools.partial(layer_body, nz, ny, nx), out_shape=jax.S...  131 us
    unnamed x3, local copies, waits for them, and re-layouts  4.5 us

profile of v6, /device:TPU:1, one launch (start us, length us, event | category | flops | bytes accessed | tf_op | source)
XLA Modules:
  0.0 135.2 jit_solution(1982415694481734120)
XLA Ops:
  0.0 1.5 %copy.16.ids_ref = s32[256,2]{1,0:T(8,128)} copy(s32[256,2]{0,1:T(2,128)} %param.25) | data formatting | bytes 4096 | tf_op args[10]
  1.5 1.5 %copy.17.rw_ref = f32[256,2]{1,0:T(8,128)} copy(f32[256,2]{0,1:T(2,128)} %param.26) | data formatting | bytes 4096 | tf_op args[11]
  2.9 130.7 %layer.1 = bf16[256,256]{1,0:T(8,128)(2,1)} custom-call(bf16[256,256]{1,0:T(8,128)(2,1)} %r_hbm.1, bf16[256,256]{1,0:T(8,128)(2,1)} %k_hbm.1, bf16[256,256]{1,0:T(8,128)(2,1)} %v_hbm.1, bf16[256,256]{1,0:T(8,128)(2,1)} %d_hbm.1, bf16[256,256]{1,0:T(8,128)(2,1)} %b_hbm.1, bf16[256,256]{1,0:T(8,128)(2,1)} %gate_hbm.1, f32[1,256]{1,0:T(1,128)} %bitcast.10, ...), custom_call_target="tpu_custom_call" | custom-call | tf_op jit(solution)/shard_map/layer/pallas_call | solution.py:782
  133.7 1.6 %copy.19 = bf16[256,256]{1,0:T(8,128)(2,1)} copy(bf16[256,256]{1,0:T(8,128)(2,1)} %layer.1) | data formatting | bytes 262144
